TPU v7x, 512 devices: a whole 4x4x16 slice. The times are simulated.
512 devices in a mesh: sp: 128 (over z, x, core), tp: 4 (over y).
Axes of the slice: x: 4, y: 4, z: 16, core: 2. Of those that a mesh axis runs over, the one named last changes fastest.
Arguments:
- tokens: bfloat16 [16384, 2048], P(('sp', 'tp')), may hold values from -6 to 6
- pre_gain: bfloat16 [2048], replicated, may hold values from 0.099609375 to 1.8984375
- w_query: bfloat16 [2048, 1024], P('sp', 'tp'), may hold values from -0.125 to 0.125
- w_key: bfloat16 [2048, 1024], P('sp', 'tp'), may hold values from -0.125 to 0.125
- w_value: bfloat16 [2048, 2048], P('sp', 'tp'), may hold values from -0.125 to 0.125
- w_igate: bfloat16 [2048, 8], replicated, may hold values from -1 to 1
- w_fgate: bfloat16 [2048, 8], replicated, may hold values from -0.125 to 0.125
- forget_bias: float32 [8], replicated, may hold values from 4 to 16
- gate_drift: float32 [16384, 8], P('sp'), may hold values from -2 to 2, as said below
- head_gain: bfloat16 [2048], replicated, may hold values from 0.099609375 to 1.8984375
- w_out: bfloat16 [2048, 2048], P('sp', 'tp'), may hold values from -0.125 to 0.125
Outputs:
- layer_out: bfloat16 [16384, 2048], P(('sp', 'tp'))
Inputs may be any that keep to these rules, and one draw needn't show every extreme that they name: `gate_drift`: constant over aligned spans of 128 positions.
All inputs are finite; a program needn't handle non-finite values.
Results may differ from a plain program's by a relative error of at most 0.02.
Values may be sent and summed in bfloat16 or wider, within the bound.
No kernel may reach another device: no remote copies, remote signals or barrier semaphores. Data moves between devices by JAX's collectives and lax.ppermute only.
A program may use at most 64 MiB of HBM per device.

v0:
```python
import jax
import jax.numpy as jnp
from jax import lax
from jax.sharding import Mesh
from jax.sharding import PartitionSpec as P

BLOCK = 64
SP = ("sp_0", "sp_1", "sp_2")
SP_TP = ("sp_0", "sp_1", "sp_2", "tp")


norm_floor = 0.1
lowest_log = -1e30
highest = lax.Precision.HIGHEST


def in_one_piece(arrays, axis, dim, along):
    widths = [a.shape[along] for a in arrays]
    both = jnp.concatenate(arrays, axis=along)
    out = lax.all_gather(both, axis, axis=dim, tiled=True)
    return tuple(jnp.split(out, [sum(widths[:k]) for k in range(1, len(widths))], axis=along))


def nothing_yet(value, identity):
    return jax.tree.map(
        lambda part, zero: jnp.zeros_like(part) + jnp.asarray(zero, part.dtype), value, identity
    )


def collected_together(value, axis):
    leaves = jax.tree.leaves(value)
    turns = sorted(range(len(leaves)), key=lambda k: -leaves[k].size)
    width = (1, *leaves[turns[0]].shape)[-1]
    lines = [
        jnp.pad(leaves[k].reshape(-1), (0, -leaves[k].size % width)).reshape(-1, width)
        for k in turns
    ]
    both, at, found = (lax.all_gather(jnp.concatenate(lines), axis), 0, {})
    for k, line in zip(turns, lines):
        slab = both[:, at : at + len(line)].reshape(len(both), -1)
        found[k] = slab[:, : leaves[k].size].reshape(-1, *leaves[k].shape)
        at += len(line)
    numbers = iter(range(len(leaves)))
    return jax.tree.map(lambda _: found[next(numbers)], value)


def carried_in(value, axes, combine, identity):
    before = start = nothing_yet(value, identity)
    subtotal = value
    for axis in reversed(axes):
        peers, position = (lax.axis_size(axis), lax.axis_index(axis))
        pieces = collected_together(
            jax.tree.map(
                lambda part, kind: part.astype(kind),
                subtotal,
                jax.tree.map(lambda a: jnp.bfloat16 if a.dtype == jnp.float32 else a.dtype, value),
            ),
            axis,
        )
        inside, subtotal = (start, start)
        for k in range(peers):
            passed = k < position
            subtotal = combine(
                subtotal, jax.tree.map(lambda part, own: part[k].astype(own.dtype), pieces, value)
            )
            inside = jax.tree.map(lambda new, old: jnp.where(passed, new, old), subtotal, inside)
        before = combine(inside, before)
    return before


def laid_out(pieces, dim):
    pieces = jnp.moveaxis(pieces, 0, dim)
    shape = pieces.shape
    return pieces.reshape(*shape[:dim], shape[dim] * shape[dim + 1], *shape[dim + 2 :])


def stacked_from(value, axes, turns):
    pieces = value
    for k in turns:
        pieces = lax.all_gather(pieces, axes[k])
    done = turns[::-1]
    back = [done.index(k) for k in range(len(axes))]
    pieces = pieces.transpose(*back, *range(len(axes), pieces.ndim))
    return pieces.reshape(-1, *value.shape)


def gather_axes(value, axes, turns, dim):
    return laid_out(stacked_from(value, axes, turns), dim)


def cut_along(value, dim, peers):
    before, after = (value.shape[:dim], value.shape[dim + 1 :])
    return jnp.moveaxis(value.reshape(*before, peers, -1, *after), dim, 0)


def sum_at_owner(value, axis, dim):
    pieces = cut_along(value, dim, lax.axis_size(axis))
    arrived = lax.all_to_all(pieces, axis, split_axis=0, concat_axis=0, tiled=True)
    return arrived.astype(jnp.float32).sum(axis=0)


def advance(memory, summary):
    old_mat, old_vec, old_top = memory
    span_log, span_top, span_mat, span_vec = summary
    new_top = jnp.maximum(span_log + old_top, span_top)
    kept_part = jnp.exp(span_log + old_top - new_top)
    fresh_part = jnp.exp(span_top - new_top)
    return (
        kept_part[:, None, None] * old_mat + fresh_part[:, None, None] * span_mat,
        kept_part[:, None] * old_vec + fresh_part[:, None] * span_vec,
        new_top,
    )


def prefix_states(initial, summary):

    def stepper(memory, one_block):
        return (advance(memory, one_block), memory)

    return lax.scan(stepper, initial, summary)


def join_devices(earlier, later_part):
    early_log, early_mat, early_vec, early_top = earlier
    late_log, late_mat, late_vec, late_top = later_part
    new_top = jnp.maximum(late_log + early_top, late_top)
    kept_part = jnp.exp(late_log + early_top - new_top)
    fresh_part = jnp.exp(late_top - new_top)
    return (
        early_log + late_log,
        kept_part[:, None, None] * early_mat + fresh_part[:, None, None] * late_mat,
        kept_part[:, None] * early_vec + fresh_part[:, None] * late_vec,
        new_top,
    )


def blend_parts(first_part, second_part):
    numer_first, denom_first, peak_first = first_part
    numer_second, denom_second, peak_second = second_part
    new_top = jnp.maximum(peak_first, peak_second)
    weight_first = jnp.exp(peak_first - new_top)
    weight_second = jnp.exp(peak_second - new_top)
    return (
        weight_first[..., None] * numer_first + weight_second[..., None] * numer_second,
        weight_first * denom_first + weight_second * denom_second,
        new_top,
    )


def on_device(
    tokens,
    pre_gain,
    w_query,
    w_key,
    w_value,
    w_igate,
    w_fgate,
    forget_bias,
    gate_drift,
    head_gain,
    w_out,
):
    tp_size = lax.axis_size("tp")
    head_count = w_igate.shape[1]
    local_heads = head_count // tp_size
    first_head = lax.axis_index("tp") * local_heads
    key_width = w_query.shape[1] // local_heads
    value_width = w_value.shape[1] // local_heads
    token_wide = tokens.astype(jnp.float32)
    scaled = token_wide * lax.rsqrt(
        jnp.mean(token_wide * token_wide, axis=1, keepdims=True) + norm_floor
    )
    normed = (scaled * pre_gain.astype(jnp.float32)).astype(jnp.bfloat16)
    gate_cols = jnp.concatenate(
        [
            lax.dynamic_slice_in_dim(w_igate, first_head, local_heads, 1),
            lax.dynamic_slice_in_dim(w_fgate, first_head, local_heads, 1),
        ],
        axis=1,
    )
    key_scale = key_width ** (-0.5)
    all_rows = lax.all_gather(normed, "tp", axis=0, tiled=True)
    pieces = in_one_piece((w_query, w_key, w_value), SP, 0, 1)
    query_sum = jnp.dot(all_rows, pieces[0], preferred_element_type=jnp.float32)
    key_sum = jnp.dot(all_rows, pieces[1], preferred_element_type=jnp.float32)
    value_sum = jnp.dot(all_rows, pieces[2], preferred_element_type=jnp.float32)
    queries = query_sum.astype(jnp.bfloat16)
    keys_all = (key_sum * key_scale).astype(jnp.bfloat16)
    values_all = value_sum.astype(jnp.bfloat16)
    gate_pre = jnp.dot(all_rows, gate_cols, preferred_element_type=jnp.float32)
    group_len = queries.shape[0]
    blocks = group_len // BLOCK
    log_input = gate_pre[:, :local_heads]
    forget_pre = gate_pre[:, local_heads:] + lax.dynamic_slice_in_dim(
        forget_bias, first_head, local_heads, 0
    )
    log_forget = jax.nn.log_sigmoid(
        forget_pre + lax.dynamic_slice_in_dim(gate_drift, first_head, local_heads, 1)
    )
    query_blk = queries.reshape(blocks, BLOCK, local_heads, key_width)
    key_blk = keys_all.reshape(blocks, BLOCK, local_heads, key_width)
    value_blk = values_all.reshape(blocks, BLOCK, local_heads, value_width)
    input_blk = log_input.reshape(blocks, BLOCK, local_heads).transpose(0, 2, 1)
    forget_blk = log_forget.reshape(blocks, BLOCK, local_heads).transpose(0, 2, 1)
    within = jnp.cumsum(forget_blk, axis=2)
    causal = jnp.arange(BLOCK)[:, None] >= jnp.arange(BLOCK)[None, :]
    log_pair = jnp.where(
        causal, within[..., :, None] - within[..., None, :] + input_blk[..., None, :], -jnp.inf
    )
    peak_intra = jnp.max(log_pair, axis=3)
    scores = jnp.einsum("nshd,nrhd->nhsr", query_blk, key_blk, preferred_element_type=jnp.float32)
    weights = scores * jnp.exp(log_pair - peak_intra[..., None])
    numer_intra = jnp.einsum(
        "nhsr,nrhv->nhsv",
        weights.astype(jnp.bfloat16),
        value_blk,
        preferred_element_type=jnp.float32,
    )
    denom_intra = jnp.sum(weights, axis=3)
    span_log = within[..., -1]
    log_write = span_log[..., None] - within + input_blk
    span_top = jnp.max(log_write, axis=2)
    write_scale = jnp.exp(log_write - span_top[..., None])
    key_scaled = key_blk.astype(jnp.float32) * write_scale.transpose(0, 2, 1)[..., None]
    value_wide = value_blk.astype(jnp.float32)
    span_mat = jnp.einsum("nrhv,nrhd->nhvd", value_wide, key_scaled, precision=highest)
    span_vec = jnp.sum(key_scaled, axis=1)
    summary = (span_log, span_top, span_mat, span_vec)
    empty_state = (
        jnp.zeros((local_heads, value_width, key_width), jnp.float32),
        jnp.zeros((local_heads, key_width), jnp.float32),
        jnp.full((local_heads,), lowest_log, jnp.float32),
    )
    local_end, local_starts = prefix_states(empty_state, summary)
    device_summary = (jnp.sum(span_log, axis=0),) + local_end
    identity_all = (jnp.zeros((local_heads,), jnp.float32),) + empty_state
    incoming = carried_in(device_summary, SP, join_devices, identity_all)
    query_wide = query_blk.astype(jnp.float32)
    intra_part = (numer_intra, denom_intra, peak_intra)
    start_mat, start_vec, start_top = local_starts
    local_part = (
        jnp.einsum("nhvd,nshd->nhsv", start_mat, query_wide, precision=highest),
        jnp.einsum("nhd,nshd->nhs", start_vec, query_wide, precision=highest),
        within + start_top[..., None],
    )
    numerator, denominator, peak_log = blend_parts(local_part, intra_part)
    entry_log, entry_mat, entry_vec, entry_top = incoming
    before_log = jnp.concatenate(
        [jnp.zeros((1, local_heads), jnp.float32), jnp.cumsum(span_log, axis=0)[:-1]], axis=0
    )
    from_left = (
        jnp.einsum("hvd,nshd->nhsv", entry_mat, query_wide, precision=highest),
        jnp.einsum("hd,nshd->nhs", entry_vec, query_wide, precision=highest),
        within + (before_log + entry_top[None, :])[..., None],
    )
    numerator, denominator, peak_log = blend_parts((numerator, denominator, peak_log), from_left)
    hidden = numerator / jnp.maximum(jnp.abs(denominator), jnp.exp(-peak_log))[..., None]
    hidden = hidden.transpose(0, 2, 1, 3).reshape(group_len, local_heads, value_width)
    head_gains = lax.dynamic_slice_in_dim(
        head_gain, first_head * value_width, local_heads * value_width, 0
    )
    head_gains = head_gains.astype(jnp.float32).reshape(local_heads, value_width)
    normed_heads = (
        hidden
        * lax.rsqrt(jnp.mean(hidden * hidden, axis=2, keepdims=True) + norm_floor)
        * head_gains
    )
    normed_heads = normed_heads.astype(jnp.bfloat16).reshape(group_len, local_heads * value_width)
    out_slab = gather_axes(w_out, SP, (1, 0, 2), 0)
    summed = sum_at_owner(
        lax.dot_general(
            normed_heads, out_slab, (((1,), (1,)), ((), ())), preferred_element_type=jnp.float32
        ).astype(jnp.bfloat16),
        "tp",
        0,
    )
    return summed.astype(jnp.bfloat16)


def solution(mesh):
    split = Mesh(mesh.devices.reshape(16, 4, 2, mesh.shape["tp"]), ("sp_0", "sp_1", "sp_2", "tp"))
    return jax.shard_map(
        on_device,
        mesh=split,
        in_specs=(
            P(SP_TP, None),
            P(),
            P(SP, "tp"),
            P(SP, "tp"),
            P(SP, "tp"),
            P(),
            P(),
            P(),
            P(SP, None),
            P(),
            P(SP, "tp"),
        ),
        out_specs=P(SP_TP, None),
        check_vma=False,
    )
```

profile of v0, /device:TPU:2, one launch (start us, length us, event | category | flops | bytes accessed | tf_op | source)
XLA Modules:
  0.0 365.4 jit_solution(10026958555231631731)
XLA Ops:
  6.5 16.8 %all-gather.3 = bf16[64,512]{1,0:T(8,128)(2,1)} all-gather(bf16[16,512]{1,0:T(8,128)(2,1)} %param.23), channel_id=5, replica_groups=mesh['sp_0'=16,'sp_1'=4,'sp_2'=2,'tp'=4] {'sp_1'}, dimensions={0}, use_global_device_ids=true | all-gather | bytes 81920 | tf_op jit(solution)/shard_map/all_gather | solution.py:80
  23.4 1.4 pad_maximum_fusion
  26.3 1.0 fusion.24
  27.3 1.0 fusion.26
  28.3 12.8 %all_gather.42 = bf16[128,2048]{1,0:T(8,128)(2,1)S(1)} all-gather(bf16[32,2048]{1,0:T(8,128)(2,1)S(1)} %fusion.26), channel_id=1, replica_groups=mesh['sp_0'=16,'sp_1'=4,'sp_2'=2,'tp'=4] {'tp'}, dimensions={0}, use_global_device_ids=true | all-gather | bytes 655360 | tf_op jit(solution)/shard_map/all_gather | solution.py:182
  41.1 0.8 constant_dynamic-slice_fusion.3
  42.2 0.8 fusion.236
  44.1 50.4 %all-gather.16.cloned.1.call-done = bf16[64,16,512]{2,1,0:T(8,128)(2,1)} async-done(((bf16[4,16,512]{2,1,0:T(8,128)(2,1)}), bf16[64,16,512]{2,1,0:T(8,128)(2,1)}) %all-gather.16.cloned.1.call-update) | async-done | bytes 1048592 | tf_op jit(solution)/shard_map/all_gather | solution.py:80
  94.5 140.9 %all-gather.14.cloned.1.call-done = bf16[2048,1024]{1,0:T(8,128)(2,1)} async-done(((bf16[16,1024]{1,0:T(8,128)(2,1)}), bf16[2048,1024]{1,0:T(8,128)(2,1)}) %all-gather.14.cloned.1.call-update) | async-done | bytes 4194320 | tf_op jit(solution)/shard_map/all_gather | solution.py:20
  235.4 1.5 fusion.21
  237.0 2.1 fusion.18
  240.5 2.0 all-gather.6
  244.5 12.5 %all-gather.7 = bf16[4,516,128]{2,1,0:T(8,128)(2,1)S(1)} all-gather(bf16[1,516,128]{2,1,0:T(8,128)(2,1)S(1)} %maximum_bitcast_fusion.1), channel_id=3, replica_groups=mesh['sp_0'=16,'sp_1'=4,'sp_2'=2,'tp'=4] {'sp_1'}, dimensions={0}, use_global_device_ids=true | all-gather | bytes 660480 | tf_op jit(solution)/shard_map/all_gather | solution.py:38
  262.7 1.8 copy.91
  264.5 2.2 convolution_convert_fusion.1
  266.7 1.5 reshape.5254
  268.2 1.6 fusion.219
  269.9 2.2 fusion.315
  272.1 0.9 slice_convert_fusion.5
  273.0 1.0 slice_convert_fusion.3
  274.0 57.8 %all-gather.20.cloned.1.call-done = bf16[16,516,128]{2,1,0:T(8,128)(2,1)} async-done(((bf16[1,516,128]{2,1,0:T(8,128)(2,1)}), bf16[16,516,128]{2,1,0:T(8,128)(2,1)}) %all-gather.20.cloned.1.call-update) | async-done | bytes 2113552 | tf_op jit(solution)/shard_map/all_gather | solution.py:38
  331.8 0.9 fusion.312
  332.7 0.9 fusion.298
  333.6 0.9 fusion.262
  334.7 1.0 fusion.240
  335.7 1.1 fusion.211
  338.2 1.1 fusion.16
  339.3 1.3 fusion.17
  340.7 1.8 fusion.311
  342.8 2.1 multiply_reduce_fusion
  345.2 0.8 convolution_convert_fusion
  346.0 12.2 %all_to_all.5 = bf16[4,32,2048]{2,1,0:T(8,128)(2,1)S(1)} all-to-all(bf16[4,32,2048]{2,1,0:T(8,128)(2,1)S(1)} %bitcast.807), channel_id=1, replica_groups=mesh['sp_0'=16,'sp_1'=4,'sp_2'=2,'tp'=4] {'tp'}, dimensions={0} | all-to-all | bytes 1048576 | tf_op jit(solution)/shard_map/all_to_all | solution.py:98
  (214 shorter events, 14.8 us)
Async XLA Ops:
  6.5 87.9 %all-gather.16.cloned.1.call-start = ((), (), s32[]{:S(2)}) async-start(), calls=%async_computation.2 | async-start | bytes 1114112 | tf_op jit(solution)/shard_map/all_gather | solution.py:80
  23.3 212.1 %all-gather.14.cloned.1.call-start = ((), (), s32[]{:S(2)}) async-start(), calls=%async_computation.1 | async-start | bytes 4227072 | tf_op jit(solution)/shard_map/all_gather | solution.py:20
  24.7 237.8 %all-gather.18.cloned.1.call-start = ((), (), s32[]{:S(2)}) async-start(), calls=%async_computation.3 | async-start | bytes 3145728 | tf_op jit(solution)/shard_map/all_gather | solution.py:80
  44.1 217.8 %copy-start.33 = (f32[2,2,64]{2,1,0:T(2,128)}, f32[2,2,64]{2,1,0:T(2,128)S(1)}, u32[]{:S(2)}) copy-start(f32[2,2,64]{2,1,0:T(2,128)S(1)} %get-tuple-element.234) | copy-start | bytes 3076
  94.5 237.4 %all-gather.20.cloned.1.call-start = ((), (), s32[]{:S(2)}) async-start(), calls=%async_computation.4 | async-start | bytes 2263040 | tf_op jit(solution)/shard_map/all_gather | solution.py:38
  237.0 2.8 copy-start
  240.4 2.3 copy-start.47
  240.4 16.8 %copy-start.48 = (f32[2,2,128]{2,1,0:T(2,128)}, f32[2,2,128]{2,1,0:T(2,128)S(1)}, u32[]{:S(2)}) copy-start(f32[2,2,128]{2,1,0:T(2,128)S(1)} %get-tuple-element.72) | copy-start | bytes 6148
  240.4 22.2 %copy-start.1 = (f32[2,2,256,128]{3,2,1,0:T(8,128)}, f32[2,2,256,128]{3,2,1,0:T(8,128)S(1)}, u32[]{:S(2)}) copy-start(f32[2,2,256,128]{3,2,1,0:T(8,128)S(1)} %get-tuple-element.71) | copy-start | bytes 1572868
  242.5 20.1 %copy-start.13 = (bf16[2,1,128]{2,0,1:T(2,128)(2,1)}, bf16[2,1,128]{2,0,1:T(2,128)(2,1)S(1)}, u32[]{:S(2)}) copy-start(bf16[2,1,128]{2,0,1:T(2,128)(2,1)S(1)} %copy.161) | copy-start | bytes 1540
  242.6 20.0 %copy-start.14 = (bf16[2,1,128]{2,0,1:T(2,128)(2,1)}, bf16[2,1,128]{2,0,1:T(2,128)(2,1)S(1)}, u32[]{:S(2)}) copy-start(bf16[2,1,128]{2,0,1:T(2,128)(2,1)S(1)} %copy.162) | copy-start | bytes 1540
  242.6 15.0 %copy-start.34 = (f32[2]{0:T(128)}, f32[2]{0:T(128)S(1)}, u32[]{:S(2)}) copy-start(f32[2]{0:T(128)S(1)} %get-tuple-element.165) | copy-start | bytes 28
  242.6 15.0 %copy-start.35 = (f32[2]{0:T(128)}, f32[2]{0:T(128)S(1)}, u32[]{:S(2)}) copy-start(f32[2]{0:T(128)S(1)} %get-tuple-element.166) | copy-start | bytes 28
  243.2 14.0 %copy-start.39 = (f32[2]{0:T(128)}, f32[2]{0:T(128)S(1)}, u32[]{:S(2)}) copy-start(f32[2]{0:T(128)S(1)} %get-tuple-element.252) | copy-start | bytes 28
  257.1 5.5 %copy-start.11 = (bf16[4,1,128]{2,0,1:T(4,128)(2,1)}, bf16[4,1,128]{2,0,1:T(4,128)(2,1)S(1)}, u32[]{:S(2)}) copy-start(bf16[4,1,128]{2,0,1:T(4,128)(2,1)S(1)} %copy.159) | copy-start | bytes 3076
  257.1 5.5 %copy-start.10 = (bf16[4,1,128]{2,0,1:T(4,128)(2,1)}, bf16[4,1,128]{2,0,1:T(4,128)(2,1)S(1)}, u32[]{:S(2)}) copy-start(bf16[4,1,128]{2,0,1:T(4,128)(2,1)S(1)} %copy.160) | copy-start | bytes 3076
  257.1 5.5 %copy-start.21 = (f32[2]{0:T(128)}, f32[2]{0:T(128)S(1)}, u32[]{:S(2)}) copy-start(f32[2]{0:T(128)S(1)} %get-tuple-element.156) | copy-start | bytes 28
  257.3 5.4 %copy-start.23 = (f32[2]{0:T(128)}, f32[2]{0:T(128)S(1)}, u32[]{:S(2)}) copy-start(f32[2]{0:T(128)S(1)} %get-tuple-element.237) | copy-start | bytes 28
  257.3 5.4 %copy-start.25 = (f32[2]{0:T(128)}, f32[2]{0:T(128)S(1)}, u32[]{:S(2)}) copy-start(f32[2]{0:T(128)S(1)} %get-tuple-element.238) | copy-start | bytes 28
  257.3 5.4 %copy-start.27 = (f32[2]{0:T(128)}, f32[2]{0:T(128)S(1)}, u32[]{:S(2)}) copy-start(f32[2]{0:T(128)S(1)} %get-tuple-element.239) | copy-start | bytes 28
  257.3 5.4 %copy-start.38 = (f32[2]{0:T(128)}, f32[2]{0:T(128)S(1)}, u32[]{:S(2)}) copy-start(f32[2]{0:T(128)S(1)} %get-tuple-element.161) | copy-start | bytes 28
  257.3 5.4 %copy-start.43 = (f32[2]{0:T(128)}, f32[2]{0:T(128)S(1)}, u32[]{:S(2)}) copy-start(f32[2]{0:T(128)S(1)} %get-tuple-element.159) | copy-start | bytes 28
  257.6 5.1 %copy-start.29 = (f32[2]{0:T(128)}, f32[2]{0:T(128)S(1)}, u32[]{:S(2)}) copy-start(f32[2]{0:T(128)S(1)} %get-tuple-element.244) | copy-start | bytes 28
  257.6 5.1 %copy-start.31 = (f32[2]{0:T(128)}, f32[2]{0:T(128)S(1)}, u32[]{:S(2)}) copy-start(f32[2]{0:T(128)S(1)} %get-tuple-element.255) | copy-start | bytes 28
  257.6 5.1 %copy-start.45 = (f32[2]{0:T(128)}, f32[2]{0:T(128)S(1)}, u32[]{:S(2)}) copy-start(f32[2]{0:T(128)S(1)} %get-tuple-element.245) | copy-start | bytes 28
  266.7 72.6 %copy-start.2 = (f32[2,2,256,128]{3,2,1,0:T(8,128)S(1)}, f32[2,2,256,128]{3,2,1,0:T(8,128)}, u32[]{:S(2)}) copy-start(f32[2,2,256,128]{3,2,1,0:T(8,128)} %copy-done.1) | copy-start | bytes 1572868
  340.5 2.0 copy-start.4
  340.6 2.0 copy-start.5
  340.6 2.0 copy-start.6
  340.6 2.0 copy-start.7
  340.6 2.0 copy-start.9
  342.8 2.1 copy-start.15
  (21 other events, 33.6 us)
Sparse Core Ops, SparseCore 0:
  23.4 70.9 all-gather.15
  97.6 137.8 all-gather.13
  237.5 18.1 all-gather.17
  260.0 71.7 all-gather.19
where the time goes:
time: 367 us; the launch traced here: 365 us
  waiting for transfers between devices  249 us (68%)
  blocking collectives  56.2 us (15%)
  other arithmetic  18.6 us (5%)
  matrix products  16.7 us (5%)
  between operations  14.2 us (4%)
  local copies, waits for them, and re-layouts  10.3 us (3%)
    all_gather x1, waiting for transfers between devices, in_one_piece(): out = lax.all_gather(both, axis, axis=dim, tiled=True)  141 us
    all_gather x1, waiting for transfers between devices, collected_together(): both, at, found = (lax.all_gather(jnp.concatenate(lines), axis), 0, {})  57.8 us
    all_gather x2, waiting for transfers between devices, stacked_from(): pieces = lax.all_gather(pieces, axes[k])  50.4 us
    all_gather x1, blocking collectives, stacked_from(): pieces = lax.all_gather(pieces, axes[k])  16.8 us
    all_gather x2, blocking collectives, collected_together(): both, at, found = (lax.all_gather(jnp.concatenate(lines), axis), 0, {})  14.5 us
    all_gather x1, blocking collectives, on_device(): all_rows = lax.all_gather(normed, 'tp', axis=0, tiled=True)  12.8 us
    all_to_all x1, blocking collectives, sum_at_owner(): lax.all_to_all(pieces, axis, split_axis=0, concat_axis=0, tiled=True)  12.2 us
  transfers between devices with their start and end apart: 4, of which 3 were waited for; matrix products, arithmetic and copies ran while one was open for 8% of the time, Pallas kernels for 0%

commit v1 on v0

v1 whole, which is shorter than its diff:
```python
import jax
import jax.numpy as jnp
from jax import lax
from jax.experimental import pallas as pl
from jax.experimental.pallas import tpu as pltpu
from jax.sharding import Mesh
from jax.sharding import PartitionSpec as P

SP = ("z", "x", "c")
SP_TP = ("z", "x", "c", "y")
ROWS = ("z", "x")
HEADS = 8
DK = 128
DV = 256
norm_floor = 0.1
lowest_log = -1e30
highest = lax.Precision.HIGHEST
f32 = jnp.float32
bf16 = jnp.bfloat16


def lane_ids(shape):
    return lax.broadcasted_iota(jnp.int32, shape, 1)


def row_ids(shape):
    return lax.broadcasted_iota(jnp.int32, shape, 0)


def prepare_kernel(tokens_ref, gain_ref, gate_w_ref, offset_ref, out_ref):
    wide = tokens_ref[...].astype(f32)
    scaled = wide * lax.rsqrt(jnp.mean(wide * wide, axis=1, keepdims=True) + norm_floor)
    normed = (scaled * gain_ref[...].astype(f32)).astype(bf16)
    width = normed.shape[1]
    out_ref[:, :width] = normed
    gates = jnp.dot(normed, gate_w_ref[...], preferred_element_type=f32)
    forget = gates + offset_ref[...]
    log_forget = jnp.minimum(forget, 0.0) - jnp.log1p(jnp.exp(-jnp.abs(forget)))
    lane = lane_ids(gates.shape)
    value = jnp.where(lane % 16 < 8, gates, log_forget)
    high = value.astype(bf16).astype(f32)
    middle = (value - high).astype(bf16).astype(f32)
    low = value - high - middle
    piece = jnp.where(lane < 16, high, jnp.where(lane < 32, middle, low))
    out_ref[:, width:] = jnp.where(lane < 48, piece, 0.0).astype(bf16)


def cell_kernel(head_ref, rows_ref, w_ref, query_ref, message_ref, numer_ref, aux_ref):
    head = head_ref[0]
    length = rows_ref.shape[0]
    width = rows_ref.shape[1] - 128
    x_size = w_ref.shape[0]
    run = width // (x_size * (w_ref.shape[1] // 32))
    total = jnp.zeros((length, w_ref.shape[2]), f32)
    for k in range(width // 256):
        parts = [
            w_ref[x, z * run : (z + 1) * run, :] for z in (2 * k, 2 * k + 1) for x in range(x_size)
        ]
        total = total + jnp.dot(
            rows_ref[:, k * 256 : (k + 1) * 256],
            jnp.concatenate(parts, axis=0),
            preferred_element_type=f32,
        )
    query = total[:, :DK].astype(bf16)
    key = (total[:, DK : 2 * DK] * (DK**-0.5)).astype(bf16)
    value = total[:, 2 * DK :].astype(bf16)
    query_ref[...] = query

    gates = rows_ref[:, width:].astype(f32)
    lane = lane_ids(gates.shape)
    input_col = jnp.sum(jnp.where(lane % 16 == head, gates, 0.0), axis=1, keepdims=True)
    forget_col = jnp.sum(jnp.where(lane % 16 == head + 8, gates, 0.0), axis=1, keepdims=True)
    both = jnp.where(lane == 0, input_col, jnp.where(lane == 1, forget_col, 0.0))
    both_rows = both.T
    input_row = both_rows[0:1, :]
    forget_row = both_rows[1:2, :]

    square = (length, length)
    s_id = row_ids(square)
    r_id = lane_ids(square)
    up_to = jnp.where(r_id <= s_id, forget_row, 0.0)
    after = jnp.where(s_id > r_id, 1.0, 0.0).astype(f32)
    decay = jnp.dot(up_to, after, precision=highest, preferred_element_type=f32)
    within = jnp.sum(up_to, axis=1, keepdims=True)
    suffix = jnp.sum(jnp.where(r_id > s_id, forget_row, 0.0), axis=1, keepdims=True)
    causal = r_id <= s_id
    log_pair = jnp.where(causal, decay + input_row, lowest_log)
    peak = jnp.max(log_pair, axis=1, keepdims=True)
    scores = lax.dot_general(query, key, (((1,), (1,)), ((), ())), preferred_element_type=f32)
    weights = jnp.where(causal, scores * jnp.exp(log_pair - peak), 0.0)
    numer_ref[...] = jnp.dot(weights.astype(bf16), value, preferred_element_type=f32)
    denom = jnp.sum(weights, axis=1, keepdims=True)
    aux_ref[...] = jnp.where(
        lane == 0, denom, jnp.where(lane == 1, peak, jnp.where(lane == 2, within, 0.0))
    )

    log_write = suffix + input_col
    top = jnp.max(log_write, axis=0, keepdims=True)
    scaled_key = key.astype(f32) * jnp.exp(log_write - top)
    state = jnp.dot(value.astype(f32).T, scaled_key, precision=highest, preferred_element_type=f32)
    vector = jnp.sum(scaled_key, axis=0, keepdims=True)
    span_log = jnp.sum(forget_row, axis=1, keepdims=True)
    peers = message_ref.shape[0] // 8
    for r in range(DV // peers):
        message_ref[pl.ds(r, peers, stride=8), :] = state[r * peers : (r + 1) * peers, :]
    small = lane_ids((peers, DK))
    message_ref[pl.ds(4, peers, stride=8), :] = jnp.broadcast_to(vector, (peers, DK))
    message_ref[pl.ds(5, peers, stride=8), :] = jnp.where(
        small == 0, span_log, jnp.where(small == 1, top, 0.0)
    )
    for r in (6, 7):
        message_ref[pl.ds(r, peers, stride=8), :] = jnp.zeros((peers, DK), f32)


def prefix_kernel(place_ref, arrived_ref, out_ref, entry_ref):
    place = place_ref[0]
    peers = arrived_ref.shape[0] // 8
    vectors = arrived_ref[pl.ds(4, peers, stride=8), :]
    facts = arrived_ref[pl.ds(5, peers, stride=8), :]
    fact_rows = facts.T
    log_row = fact_rows[0:1, :]
    top_row = fact_rows[1:2, :]
    square = (peers, peers)
    i_id = row_ids(square)
    j_id = lane_ids(square)
    before = jnp.where(j_id < i_id, log_row, 0.0)
    after = jnp.where(i_id > j_id, 1.0, 0.0).astype(f32)
    logs = jnp.dot(before, after, precision=highest, preferred_element_type=f32) + top_row
    earlier = j_id < i_id
    logs = jnp.where(earlier, logs, lowest_log)
    top = jnp.max(logs, axis=1, keepdims=True)
    mix = jnp.where(earlier, jnp.exp(logs - top), 0.0)
    count = out_ref.shape[0] // peers
    for r in range(count):
        out_ref[pl.ds(r, peers, stride=count), :] = jnp.dot(
            mix,
            arrived_ref[pl.ds(r, peers, stride=8), :],
            precision=highest,
            preferred_element_type=f32,
        )
    entries = jnp.dot(mix, vectors, precision=highest, preferred_element_type=f32)
    mine = row_ids(entries.shape) == place
    vector = jnp.sum(jnp.where(mine, entries, 0.0), axis=0, keepdims=True)
    entry_top = jnp.sum(jnp.where(mine, top, 0.0), axis=0, keepdims=True)
    row = row_ids(entry_ref.shape)
    entry_ref[...] = jnp.where(row == 0, vector, jnp.where(row == 1, entry_top, 0.0))


def finish_kernel(
    head_ref, query_ref, numer_ref, aux_ref, state_ref, entry_ref, gain_ref, w_ref, out_ref
):
    head = head_ref[0]
    count = DV * DK // (state_ref.shape[1] * 64)
    peers = state_ref.shape[0] // count
    state = jnp.concatenate(
        [state_ref[pl.ds(r, peers, stride=count), :] for r in range(count)], axis=0
    )
    query = query_ref[...].astype(f32)
    left = lax.dot_general(
        query, state, (((1,), (1,)), ((), ())), precision=highest, preferred_element_type=f32
    )
    entry_vec = entry_ref[0:1, :]
    entry_top = entry_ref[1:2, 0:1]
    left_denom = jnp.sum(query * entry_vec, axis=1, keepdims=True)
    aux = aux_ref[...]
    lane = lane_ids(aux.shape)
    denom = jnp.sum(jnp.where(lane == 0, aux, 0.0), axis=1, keepdims=True)
    peak = jnp.sum(jnp.where(lane == 1, aux, 0.0), axis=1, keepdims=True)
    within = jnp.sum(jnp.where(lane == 2, aux, 0.0), axis=1, keepdims=True)
    carried = within + entry_top
    top = jnp.maximum(peak, carried)
    own = jnp.exp(peak - top)
    old = jnp.exp(carried - top)
    numer = own * numer_ref[...] + old * left
    denom = own * denom + old * left_denom
    hidden = numer / jnp.maximum(jnp.abs(denom), jnp.exp(-top))
    gains = gain_ref[...].astype(f32)
    gain = jnp.sum(jnp.where(row_ids(gains.shape) == head, gains, 0.0), axis=0, keepdims=True)
    scale = lax.rsqrt(jnp.mean(hidden * hidden, axis=1, keepdims=True) + norm_floor)
    heads_out = (hidden * scale * gain).astype(bf16)
    x_size = w_ref.shape[0]
    run = 32
    for k in range(out_ref.shape[1] // 256):
        parts = [
            w_ref[x, z * run : (z + 1) * run, :] for z in (2 * k, 2 * k + 1) for x in range(x_size)
        ]
        out_ref[:, k * 256 : (k + 1) * 256] = lax.dot_general(
            heads_out,
            jnp.concatenate(parts, axis=0),
            (((1,), (1,)), ((), ())),
            preferred_element_type=f32,
        ).astype(bf16)


def on_device(
    tokens,
    pre_gain,
    w_query,
    w_key,
    w_value,
    w_igate,
    w_fgate,
    forget_bias,
    gate_drift,
    head_gain,
    w_out,
):
    width = tokens.shape[1]
    z_size, x_size = lax.axis_size("z"), lax.axis_size("x")
    peers = z_size * x_size
    head = (lax.axis_index("y") * 2 + lax.axis_index("c")).astype(jnp.int32).reshape(1)
    place = (lax.axis_index("z") * x_size + lax.axis_index("x")).astype(jnp.int32).reshape(1)
    smem = pl.BlockSpec(memory_space=pltpu.SMEM)
    vmem = pl.BlockSpec(memory_space=pltpu.VMEM)

    gate_w = jnp.concatenate([w_igate, w_fgate] * 3 + [jnp.zeros((width, 80), bf16)], axis=1)
    offsets = jnp.concatenate([jnp.zeros((8,), f32), forget_bias + gate_drift[0]] * 3)
    offsets = jnp.pad(offsets, (0, 80)).reshape(1, 128)
    rows = tokens.shape[0]
    own_rows = pl.pallas_call(
        prepare_kernel,
        out_shape=jax.ShapeDtypeStruct((rows, width + 128), bf16),
        in_specs=[vmem] * 4,
        out_specs=vmem,
        name="prepare",
    )(tokens, pre_gain.reshape(1, width), gate_w, offsets)
    all_rows = lax.all_gather(own_rows, ("c", "y"), axis=0, tiled=True)

    pair = jnp.stack(
        [
            jnp.concatenate(
                [
                    w_query[:, c * DK : (c + 1) * DK],
                    w_key[:, c * DK : (c + 1) * DK],
                    w_value[:, c * DV : (c + 1) * DV],
                    w_out[:, c * DV : (c + 1) * DV],
                ],
                axis=1,
            )
            for c in range(2)
        ]
    )
    mine = lax.all_to_all(pair, "c", split_axis=0, concat_axis=0, tiled=True)
    mine = mine.reshape(-1, mine.shape[2])
    along_z = lax.all_gather(mine, "z", axis=0, tiled=True)
    cut = 2 * DK + DV
    out_part = along_z[:, cut:]
    in_part = along_z[:, :cut]
    w_in = lax.all_to_all(
        jnp.broadcast_to(in_part[None], (x_size,) + in_part.shape),
        "x",
        split_axis=0,
        concat_axis=0,
        tiled=True,
    )
    w_back = lax.all_gather(out_part, "x", axis=0, tiled=False)

    length = all_rows.shape[0]
    query, message, numer, aux = pl.pallas_call(
        cell_kernel,
        out_shape=(
            jax.ShapeDtypeStruct((length, DK), bf16),
            jax.ShapeDtypeStruct((peers * 8, DK), f32),
            jax.ShapeDtypeStruct((length, DV), f32),
            jax.ShapeDtypeStruct((length, 128), f32),
        ),
        in_specs=[smem, vmem, vmem],
        out_specs=(vmem,) * 4,
        name="cell",
    )(head, all_rows, w_in)
    arrived = lax.all_to_all(message, ROWS, split_axis=0, concat_axis=0, tiled=True)
    slices, entry = pl.pallas_call(
        prefix_kernel,
        out_shape=(
            jax.ShapeDtypeStruct((DV, DK), f32),
            jax.ShapeDtypeStruct((8, 128), f32),
        ),
        in_specs=[smem, vmem],
        out_specs=(vmem,) * 2,
        name="prefix",
    )(place, arrived)
    state = lax.all_to_all(slices, ROWS, split_axis=0, concat_axis=0, tiled=True)
    partial = pl.pallas_call(
        finish_kernel,
        out_shape=jax.ShapeDtypeStruct((length, width), bf16),
        in_specs=[smem] + [vmem] * 7,
        out_specs=vmem,
        name="finish",
    )(head, query, numer, aux, state, entry, head_gain.reshape(HEADS, DV), w_back)
    pieces = lax.all_to_all(
        partial.reshape(-1, rows, width), ("c", "y"), split_axis=0, concat_axis=0, tiled=True
    )
    return pieces.astype(f32).sum(axis=0).astype(bf16)


def solution(mesh):
    split = Mesh(mesh.devices.reshape(16, 4, 2, mesh.shape["tp"]), ("z", "x", "c", "y"))
    return jax.shard_map(
        on_device,
        mesh=split,
        in_specs=(
            P(SP_TP, None),
            P(),
            P(SP, "y"),
            P(SP, "y"),
            P(SP, "y"),
            P(),
            P(),
            P(),
            P(SP, None),
            P(),
            P(SP, "y"),
        ),
        out_specs=P(SP_TP, None),
        check_vma=False,
    )
```

time: 367 us -> 177 us (0.48)
  the two profiles are of different devices: /device:TPU:2 before, /device:TPU:1 now
where the time goes in v1:
time: 177 us; the launch traced here: 176 us
  blocking collectives  68.2 us (39%)
  waiting for transfers between devices  50.6 us (29%)
  starting transfers between devices  16.6 us (9%)
  between operations  13.6 us (8%)
  local copies, waits for them, and re-layouts  12.9 us (7%)
  Pallas kernels  12.6 us (7%)
    all_to_all x1, blocking collectives, on_device(): lax.all_to_all(partial.reshape(-1, rows, width), ('c', 'y'), split_axis=0...  29.7 us
    all_gather x1, blocking collectives, on_device(): along_z = lax.all_gather(mine, 'z', axis=0, tiled=True)  28.3 us
    all_to_all x1, waiting for transfers between devices, on_device(): lax.all_to_all(jnp.broadcast_to(in_part[None], (x_size,) + in_part.shape)...  18.6 us
    all_to_all x1, waiting for transfers between devices, on_device(): lax.all_to_all(message, ROWS, split_axis=0, concat_axis=0, tiled=True)  17.5 us
    all_to_all x1, waiting for transfers between devices, on_device(): lax.all_to_all(slices, ROWS, split_axis=0, concat_axis=0, tiled=True)  14.5 us
    all_to_all x1, blocking collectives, on_device(): mine = lax.all_to_all(pair, 'c', split_axis=0, concat_axis=0, tiled=True)  10.3 us
    all_to_all x1, starting transfers between devices, on_device(): lax.all_to_all(message, ROWS, split_axis=0, concat_axis=0, tiled=True)  7.98 us
    unnamed x18, local copies, waits for them, and re-layouts  4.77 us
  transfers between devices with their start and end apart: 5, of which 3 were waited for; matrix products, arithmetic and copies ran while one was open for 2% of the time, Pallas kernels for 4%

profile of v1, /device:TPU:1, one launch (start us, length us, event | category | flops | bytes accessed | tf_op | source)
XLA Modules:
  0.0 176.0 jit_solution(3190243039448284990)
XLA Ops:
  6.5 1.0 copy.12
  7.6 1.0 copy.13
  8.6 1.3 reshape.27.gain_ref
  9.9 0.8 slice_reduce_fusion
  10.7 0.7 add.12
  11.4 0.1 concatenate.13
  11.4 0.5 pad_bitcast_fusion.offset_ref
  12.0 0.1 broadcast_in_dim.4
  12.1 0.0 copy-start.5
  12.1 2.5 %concatenate.12.gate_w_ref = bf16[2048,128]{1,0:T(8,128)(2,1)} concatenate(bf16[2048,8]{1,0:T(8,128)(2,1)S(1)} %copy.12, bf16[2048,8]{1,0:T(8,128)(2,1)S(1)} %copy.13, bf16[2048,8]{1,0:T(8,128)(2,1)S(1)} %copy.12, bf16[2048,8]{1,0:T(8,128)(2,1)S(1)} %copy.13, bf16[2048,8]{1,0:T(8,128)(2,1)S(1)} %copy.12, bf16[2048,8]{1,0:T(8,128)(2,1)S(1)} %copy.13, ...), dimensions={1} | concatenate | bytes 1048576 | tf_op jit(solution)/shard_map/concatenate | solution.py:216
  14.5 2.1 %prepare.1 = bf16[32,2176]{1,0:T(8,128)(2,1)} custom-call(bf16[32,2048]{1,0:T(8,128)(2,1)} %tokens_ref.1, bf16[1,2048]{1,0:T(2,128)(2,1)} %reshape.27.gain_ref, bf16[2048,128]{1,0:T(8,128)(2,1)} %concatenate.12.gate_w_ref, f32[1,128]{1,0:T(1,128)} %pad_bitcast_fusion.offset_ref), custom_call_target="tpu_custom_call" | custom-call | tf_op jit(solution)/shard_map/prepare/pallas_call | solution.py:220
  16.6 0.0 all-gather.4.cloned.1.call-update
  16.8 10.3 %all_to_all.37 = bf16[2,16,768]{2,1,0:T(8,128)(2,1)S(1)} all-to-all(bf16[2,16,768]{2,1,0:T(8,128)(2,1)S(1)} %pad_maximum_fusion), channel_id=1, replica_groups=mesh['z'=16,'x'=4,'c'=2,'y'=4] {'c'}, dimensions={0} | all-to-all | bytes 98304 | tf_op jit(solution)/shard_map/all_to_all | solution.py:243
  27.0 28.3 %all_gather.13 = bf16[512,768]{1,0:T(8,128)(2,1)S(1)} all-gather(bf16[32,768]{1,0:T(8,128)(2,1)S(1)} %bitcast.20), channel_id=1, replica_groups=mesh['z'=16,'x'=4,'c'=2,'y'=4] {'z'}, dimensions={0}, use_global_device_ids=true | all-gather | bytes 835584 | tf_op jit(solution)/shard_map/all_gather | solution.py:245
  55.4 1.5 broadcast_in_dim.10
  56.9 4.0 %all-to-all-start.1 = ((bf16[4,512,512]{2,1,0:T(8,128)(2,1)}), bf16[4,512,512]{2,1,0:T(8,128)(2,1)S(1)}, u32[]{:S(2)}, u32[]{:S(2)}) async-start(bf16[4,512,512]{2,1,0:T(8,128)(2,1)} %broadcast_in_dim.10), calls=%async_computation.1 | async-start | bytes 4194304 | tf_op jit(solution)/shard_map/all_to_all | solution.py:249
  60.9 0.7 slice.45
  61.6 0.0 all-gather.6.cloned.1.call-update
  61.7 18.6 %all-to-all-done.1.w_ref = bf16[4,512,512]{2,1,0:T(8,128)(2,1)S(1)} async-done(((bf16[4,512,512]{2,1,0:T(8,128)(2,1)}), bf16[4,512,512]{2,1,0:T(8,128)(2,1)S(1)}, u32[]{:S(2)}, u32[]{:S(2)}) %all-to-all-start.1) | async-done | bytes 2097184 | tf_op jit(solution)/shard_map/all_to_all | solution.py:249
  80.3 1.3 copy-done
  81.6 4.6 %cell.1 = (bf16[256,128]{1,0:T(8,128)(2,1)}, f32[512,128]{1,0:T(8,128)}, f32[256,256]{1,0:T(8,128)}, f32[256,128]{1,0:T(8,128)}) custom-call(s32[1]{0:T(128)} %bitcast.head_ref, bf16[256,2176]{1,0:T(8,128)(2,1)} %all-gather.4.cloned.1.call-done.rows_ref, bf16[4,512,512]{2,1,0:T(8,128)(2,1)} %copy-done), custom_call_target="tpu_custom_call" | custom-call | tf_op jit(solution)/shard_map/cell/pallas_call | solution.py:259
  86.2 8.0 %all-to-all-start.2 = ((f32[64,8,128]{2,1,0:T(8,128)}), f32[64,8,128]{2,1,0:T(8,128)S(1)}, u32[]{:S(2)}, u32[]{:S(2)}) async-start(f32[64,8,128]{2,1,0:T(8,128)} %bitcast.19), calls=%async_computation.2 | async-start | bytes 524288 | tf_op jit(solution)/shard_map/all_to_all | solution.py:271
  94.2 17.5 %all-to-all-done.2 = f32[64,8,128]{2,1,0:T(8,128)S(1)} async-done(((f32[64,8,128]{2,1,0:T(8,128)}), f32[64,8,128]{2,1,0:T(8,128)S(1)}, u32[]{:S(2)}, u32[]{:S(2)}) %all-to-all-start.2) | async-done | bytes 262176 | tf_op jit(solution)/shard_map/all_to_all | solution.py:271
  111.7 0.7 copy-done.1
  112.4 2.2 %prefix.1 = (f32[256,128]{1,0:T(8,128)}, f32[8,128]{1,0:T(8,128)}) custom-call(s32[1]{0:T(128)} %bitcast.5.place_ref, f32[512,128]{1,0:T(8,128)} %bitcast.17), custom_call_target="tpu_custom_call" | custom-call | tf_op jit(solution)/shard_map/prefix/pallas_call | solution.py:272
  114.5 4.6 %all-to-all-start.3 = ((f32[64,4,128]{2,1,0:T(4,128)}), f32[64,4,128]{2,1,0:T(4,128)S(1)}, u32[]{:S(2)}, u32[]{:S(2)}) async-start(f32[64,4,128]{2,1,0:T(4,128)} %bitcast.21), calls=%async_computation.3 | async-start | bytes 262144 | tf_op jit(solution)/shard_map/all_to_all | solution.py:282
  119.1 0.6 reshape.31.gain_ref
  119.7 14.5 %all-to-all-done.3 = f32[64,4,128]{2,1,0:T(4,128)S(1)} async-done(((f32[64,4,128]{2,1,0:T(4,128)}), f32[64,4,128]{2,1,0:T(4,128)S(1)}, u32[]{:S(2)}, u32[]{:S(2)}) %all-to-all-start.3) | async-done | bytes 131104 | tf_op jit(solution)/shard_map/all_to_all | solution.py:282
  134.3 0.7 copy-done.2
  134.9 3.7 %finish.1 = bf16[256,2048]{1,0:T(8,128)(2,1)} custom-call(s32[1]{0:T(128)} %bitcast.head_ref, bf16[256,128]{1,0:T(8,128)(2,1)} %get-tuple-element.11.query_ref, f32[256,256]{1,0:T(8,128)} %get-tuple-element.12.numer_ref, f32[256,128]{1,0:T(8,128)} %get-tuple-element.13.aux_ref, f32[256,128]{1,0:T(8,128)} %bitcast.18, f32[8,128]{1,0:T(8,128)} %get-tuple-element.16.entry_ref, ...), custom_call_target="tpu_custom_call" | custom-call | tf_op jit(solution)/shard_map/finish/pallas_call | solution.py:283
  138.7 29.7 %all_to_all.38 = bf16[8,32,2048]{2,1,0:T(8,128)(2,1)S(1)} all-to-all(bf16[8,32,2048]{2,1,0:T(8,128)(2,1)} %bitcast.15), channel_id=1, replica_groups=mesh['z'=16,'x'=4,'c'=2,'y'=4] {'c','y'}, dimensions={0} | all-to-all | bytes 2097152 | tf_op jit(solution)/shard_map/all_to_all | solution.py:290
  168.3 0.8 reduce_sum.12
  (24 shorter events, 0.1 us)
Async XLA Ops:
  6.5 73.7 %all-gather.4.cloned.1.call-start = ((), (), s32[]{:S(2)}) async-start(), calls=%async_computation.5 | async-start | bytes 1253376 | tf_op jit(solution)/shard_map/all_gather | solution.py:227
  12.0 4.6 %copy-start.3 = (bf16[16,512]{1,0:T(8,128)(2,1)S(1)}, bf16[16,512]{1,0:T(8,128)(2,1)}, u32[]{:S(2)}) copy-start(bf16[16,512]{1,0:T(8,128)(2,1)} %param.15) | copy-start | bytes 49156
  12.0 4.6 %copy-start.4 = (bf16[16,512]{1,0:T(8,128)(2,1)S(1)}, bf16[16,512]{1,0:T(8,128)(2,1)}, u32[]{:S(2)}) copy-start(bf16[16,512]{1,0:T(8,128)(2,1)} %param.21) | copy-start | bytes 49156
  12.1 4.7 %copy-start.5 = (bf16[16,256]{1,0:T(8,128)(2,1)S(1)}, bf16[16,256]{1,0:T(8,128)(2,1)}, u32[]{:S(2)}) copy-start(bf16[16,256]{1,0:T(8,128)(2,1)} %param.13) | copy-start | bytes 24580
  12.1 4.7 %copy-start.6 = (bf16[16,256]{1,0:T(8,128)(2,1)S(1)}, bf16[16,256]{1,0:T(8,128)(2,1)}, u32[]{:S(2)}) copy-start(bf16[16,256]{1,0:T(8,128)(2,1)} %param.14) | copy-start | bytes 24580
  56.9 23.4 %all-to-all-start.1 = ((bf16[4,512,512]{2,1,0:T(8,128)(2,1)}), bf16[4,512,512]{2,1,0:T(8,128)(2,1)S(1)}, u32[]{:S(2)}, u32[]{:S(2)}) async-start(bf16[4,512,512]{2,1,0:T(8,128)(2,1)} %broadcast_in_dim.10), calls=%async_computation.1 | async-start | bytes 4194304 | tf_op jit(solution)/shard_map/all_to_all | solution.py:249
  60.9 58.9 %all-gather.6.cloned.1.call-start = ((), (), s32[]{:S(2)}) async-start(), calls=%async_computation.6 | async-start | bytes 1310720 | tf_op jit(solution)/shard_map/all_gather | solution.py:256
  80.2 1.3 copy-start
  81.6 37.5 %copy-start.7 = (bf16[2048]{0:T(1024)(128)(2,1)S(1)}, bf16[2048]{0:T(1024)(128)(2,1)}, u32[]{:S(2)}) copy-start(bf16[2048]{0:T(1024)(128)(2,1)} %param.20) | copy-start | bytes 12292
  86.2 25.5 %all-to-all-start.2 = ((f32[64,8,128]{2,1,0:T(8,128)}), f32[64,8,128]{2,1,0:T(8,128)S(1)}, u32[]{:S(2)}, u32[]{:S(2)}) async-start(f32[64,8,128]{2,1,0:T(8,128)} %bitcast.19), calls=%async_computation.2 | async-start | bytes 524288 | tf_op jit(solution)/shard_map/all_to_all | solution.py:271
  111.7 0.7 copy-start.1
  114.5 19.8 %all-to-all-start.3 = ((f32[64,4,128]{2,1,0:T(4,128)}), f32[64,4,128]{2,1,0:T(4,128)S(1)}, u32[]{:S(2)}, u32[]{:S(2)}) async-start(f32[64,4,128]{2,1,0:T(4,128)} %bitcast.21), calls=%async_computation.3 | async-start | bytes 262144 | tf_op jit(solution)/shard_map/all_to_all | solution.py:282
  134.3 0.7 copy-start.2
Sparse Core Ops, SparseCore 0:
  16.8 36.8 all-gather.3
  63.8 32.6 all-gather.5

commit v2 on v1

v2 whole, which is shorter than its diff:
```python
import jax
import jax.numpy as jnp
from jax import lax
from jax.experimental import pallas as pl
from jax.experimental.pallas import tpu as pltpu
from jax.sharding import Mesh
from jax.sharding import PartitionSpec as P

SP = ("z", "x", "c")
SP_TP = ("z", "x", "c", "y")
ROWS = ("z", "x")
HEADS = 8
DK = 128
DV = 256
norm_floor = 0.1
lowest_log = -1e30
highest = lax.Precision.HIGHEST
f32 = jnp.float32
bf16 = jnp.bfloat16


def near(array):
    return pltpu.with_memory_space_constraint(array, pltpu.VMEM)


def lane_ids(shape):
    return lax.broadcasted_iota(jnp.int32, shape, 1)


def row_ids(shape):
    return lax.broadcasted_iota(jnp.int32, shape, 0)


def three_parts(value):
    high = value.astype(bf16).astype(f32)
    middle = (value - high).astype(bf16).astype(f32)
    return high, middle, value - high - middle


def prepare_kernel(bias_ref, tokens_ref, gain_ref, w_igate_ref, w_fgate_ref, drift_ref, out_ref):
    wide = tokens_ref[...].astype(f32)
    scale = lax.rsqrt(jnp.mean(wide * wide, axis=1, keepdims=True) + norm_floor)
    gain = gain_ref[...].astype(f32)
    blocks = gain.shape[0]
    normed = jnp.concatenate(
        [
            (wide[:, k * 128 : (k + 1) * 128] * scale * gain[k : k + 1, :]).astype(bf16)
            for k in range(blocks)
        ],
        axis=1,
    )
    width = normed.shape[1]
    across = (((1,), (1,)), ((), ()))
    gate_in = lax.dot_general(w_igate_ref[...], normed, across, preferred_element_type=f32)
    forget = lax.dot_general(w_fgate_ref[...], normed, across, preferred_element_type=f32)
    heads = forget.shape[0]
    line = row_ids((heads, 1))
    bias = jnp.zeros((heads, 1), f32)
    for h in range(heads):
        bias = jnp.where(line == h, bias_ref[h], bias)
    forget = forget + bias + drift_ref[:, 0:1]
    log_forget = jnp.minimum(forget, 0.0) - jnp.log1p(jnp.exp(-jnp.abs(forget)))
    lane = lane_ids((heads, 128))
    row = row_ids((heads, 128))
    place_in = jnp.where(lane % 16 == row, 1.0, 0.0).astype(f32)
    place_forget = jnp.where(lane % 16 == row + heads, 1.0, 0.0).astype(f32)
    value = jnp.dot(
        gate_in.T, place_in, precision=highest, preferred_element_type=f32
    ) + jnp.dot(log_forget.T, place_forget, precision=highest, preferred_element_type=f32)
    high, middle, low = three_parts(value)
    lane = lane_ids(value.shape)
    piece = jnp.where(lane < 16, high, jnp.where(lane < 32, middle, low))
    piece = jnp.where(lane < 48, piece, 0.0).astype(bf16)
    for k in range(out_ref.shape[0]):
        out_ref[k, :, :width] = normed
        out_ref[k, :, width:] = piece


def gates_kernel(head_ref, rows_ref, pair_ref, aux_ref, facts_ref):
    head = head_ref[0]
    gates = rows_ref[:, -128:].astype(f32)
    length = gates.shape[0]
    lane = lane_ids(gates.shape)
    input_col = jnp.sum(jnp.where(lane % 16 == head, gates, 0.0), axis=1, keepdims=True)
    forget_col = jnp.sum(jnp.where(lane % 16 == head + 8, gates, 0.0), axis=1, keepdims=True)
    both = jnp.where(lane == 0, input_col, jnp.where(lane == 1, forget_col, 0.0))
    both_rows = both.T
    input_row = both_rows[0:1, :]
    forget_row = both_rows[1:2, :]
    square = (length, length)
    s_id = row_ids(square)
    r_id = lane_ids(square)
    causal = r_id <= s_id
    up_to = jnp.where(causal, forget_row, 0.0)
    after = jnp.where(s_id > r_id, 1.0, 0.0).astype(f32)
    decay = jnp.dot(up_to, after, precision=highest, preferred_element_type=f32)
    within = jnp.sum(up_to, axis=1, keepdims=True)
    suffix = jnp.sum(jnp.where(r_id > s_id, forget_row, 0.0), axis=1, keepdims=True)
    log_pair = jnp.where(causal, decay + input_row, lowest_log)
    peak = jnp.max(log_pair, axis=1, keepdims=True)
    pair_ref[...] = jnp.where(causal, jnp.exp(log_pair - peak), 0.0)
    log_write = suffix + input_col
    top = jnp.max(log_write, axis=0, keepdims=True)
    write = jnp.exp(log_write - top)
    aux_ref[...] = jnp.where(
        lane == 1, peak, jnp.where(lane == 2, within, jnp.where(lane == 3, write, 0.0))
    )
    span_log = jnp.sum(forget_row, axis=1, keepdims=True)
    small = lane_ids(facts_ref.shape)
    facts = jnp.zeros(facts_ref.shape, f32)
    for k, piece in enumerate(three_parts(span_log) + three_parts(top)):
        facts = jnp.where(small == k, piece, facts)
    facts_ref[...] = facts


def column_of(aux, k):
    return jnp.sum(jnp.where(lane_ids(aux.shape) == k, aux, 0.0), axis=1, keepdims=True)


def state_kernel(
    rows_ref, w_ref, aux_ref, facts_ref, query_ref, key_ref, value_ref, message_ref, buffer_ref
):
    length, width = rows_ref.shape[0], rows_ref.shape[1] - 128
    x_size = w_ref.shape[0]
    run = 32
    total = jnp.zeros((length, w_ref.shape[2]), f32)
    for k in range(width // 256):
        parts = [
            w_ref[x, z * run : (z + 1) * run, :] for z in (2 * k, 2 * k + 1) for x in range(x_size)
        ]
        total = total + jnp.dot(
            rows_ref[:, k * 256 : (k + 1) * 256],
            jnp.concatenate(parts, axis=0),
            preferred_element_type=f32,
        )
    query_ref[...] = total[:, :DK].astype(bf16)
    key = (total[:, DK : 2 * DK] * (DK**-0.5)).astype(bf16)
    value = total[:, 2 * DK :].astype(bf16)
    key_ref[...] = key
    value_ref[...] = value
    scaled_key = key.astype(f32) * column_of(aux_ref[...], 3)
    state = jnp.dot(value.astype(f32).T, scaled_key, precision=highest, preferred_element_type=f32)
    vector = jnp.sum(scaled_key, axis=0, keepdims=True)
    peers = buffer_ref.shape[0] // 8
    for r in range(DV // peers):
        buffer_ref[pl.ds(r, peers, stride=8), :] = state[r * peers : (r + 1) * peers, :]
    buffer_ref[pl.ds(4, peers, stride=8), :] = jnp.broadcast_to(vector, (peers, DK))
    buffer_ref[pl.ds(5, peers, stride=8), :] = jnp.broadcast_to(facts_ref[0:1, :], (peers, DK))
    for r in (6, 7):
        buffer_ref[pl.ds(r, peers, stride=8), :] = jnp.zeros((peers, DK), f32)
    message_ref[...] = buffer_ref[...].astype(bf16)


def intra_kernel(query_ref, key_ref, value_ref, pair_ref, numer_ref, denom_ref):
    scores = lax.dot_general(
        query_ref[...], key_ref[...], (((1,), (1,)), ((), ())), preferred_element_type=f32
    )
    weights = scores * pair_ref[...]
    numer_ref[...] = jnp.dot(weights.astype(bf16), value_ref[...], preferred_element_type=f32)
    denom = jnp.sum(weights, axis=1, keepdims=True)
    denom_ref[...] = jnp.broadcast_to(denom, denom_ref.shape)


def prefix_kernel(place_ref, arrived_ref, out_ref, entry_ref, buffer_ref):
    place = place_ref[0]
    buffer_ref[...] = arrived_ref[...].astype(f32)
    peers = buffer_ref.shape[0] // 8
    vectors = buffer_ref[pl.ds(4, peers, stride=8), :]
    fact_rows = buffer_ref[pl.ds(5, peers, stride=8), :].T
    log_row = fact_rows[0:1, :] + fact_rows[1:2, :] + fact_rows[2:3, :]
    top_row = fact_rows[3:4, :] + fact_rows[4:5, :] + fact_rows[5:6, :]
    square = (peers, peers)
    i_id = row_ids(square)
    j_id = lane_ids(square)
    earlier = j_id < i_id
    before = jnp.where(earlier, log_row, 0.0)
    after = jnp.where(i_id > j_id, 1.0, 0.0).astype(f32)
    logs = jnp.dot(before, after, precision=highest, preferred_element_type=f32) + top_row
    logs = jnp.where(earlier, logs, lowest_log)
    top = jnp.max(logs, axis=1, keepdims=True)
    mix = jnp.where(earlier, jnp.exp(logs - top), 0.0)
    count = out_ref.shape[0] // peers
    for r in range(count):
        out_ref[pl.ds(r, peers, stride=count), :] = jnp.dot(
            mix,
            buffer_ref[pl.ds(r, peers, stride=8), :],
            precision=highest,
            preferred_element_type=f32,
        )
    entries = jnp.dot(mix, vectors, precision=highest, preferred_element_type=f32)
    mine = row_ids(entries.shape) == place
    vector = jnp.sum(jnp.where(mine, entries, 0.0), axis=0, keepdims=True)
    entry_top = jnp.sum(jnp.where(mine, top, 0.0), axis=0, keepdims=True)
    row = row_ids(entry_ref.shape)
    entry_ref[...] = jnp.where(row == 0, vector, jnp.where(row == 1, entry_top, 0.0))


def finish_kernel(
    head_ref,
    query_ref,
    numer_ref,
    denom_ref,
    aux_ref,
    state_ref,
    entry_ref,
    gain_ref,
    w_0_ref,
    w_1_ref,
    w_2_ref,
    w_3_ref,
    out_ref,
    w_ref,
):
    head = head_ref[0]
    my_x = head_ref[1]
    for d, piece_ref in enumerate((w_0_ref, w_1_ref, w_2_ref, w_3_ref)):
        w_ref[(my_x + 4 - d) % 4] = piece_ref[...]
    peers = 64
    count = state_ref.shape[0] // peers
    state = jnp.concatenate(
        [state_ref[pl.ds(r, peers, stride=count), :] for r in range(count)], axis=0
    )
    query = query_ref[...].astype(f32)
    left = lax.dot_general(
        query, state, (((1,), (1,)), ((), ())), precision=highest, preferred_element_type=f32
    )
    entry_vec = entry_ref[0:1, :]
    entry_top = entry_ref[1:2, 0:1]
    left_denom = jnp.sum(query * entry_vec, axis=1, keepdims=True)
    aux = aux_ref[...]
    denom = denom_ref[:, 0:1]
    peak = column_of(aux, 1)
    carried = column_of(aux, 2) + entry_top
    top = jnp.maximum(peak, carried)
    own = jnp.exp(peak - top)
    old = jnp.exp(carried - top)
    numer = own * numer_ref[...] + old * left
    denom = own * denom + old * left_denom
    hidden = numer / jnp.maximum(jnp.abs(denom), jnp.exp(-top))
    gains = gain_ref[...].astype(f32)
    row = row_ids(gains.shape)
    gain = jnp.concatenate(
        [
            jnp.sum(jnp.where(row == 2 * head + k, gains, 0.0), axis=0, keepdims=True)
            for k in range(2)
        ],
        axis=1,
    )
    scale = lax.rsqrt(jnp.mean(hidden * hidden, axis=1, keepdims=True) + norm_floor)
    heads_out = (hidden * scale * gain).astype(bf16)
    x_size = w_ref.shape[0]
    run = 32
    for k in range(out_ref.shape[1] // 256):
        parts = [
            w_ref[x, z * run : (z + 1) * run, :] for z in (2 * k, 2 * k + 1) for x in range(x_size)
        ]
        out_ref[:, k * 256 : (k + 1) * 256] = lax.dot_general(
            heads_out,
            jnp.concatenate(parts, axis=0),
            (((1,), (1,)), ((), ())),
            preferred_element_type=f32,
        ).astype(bf16)


def on_device(
    tokens,
    pre_gain,
    w_query,
    w_key,
    w_value,
    w_igate,
    w_fgate,
    forget_bias,
    gate_drift,
    head_gain,
    w_out,
):
    rows, width = tokens.shape
    z_size, x_size = lax.axis_size("z"), lax.axis_size("x")
    peers = z_size * x_size
    core = lax.axis_index("c")
    head = (lax.axis_index("y") * 2 + core).astype(jnp.int32).reshape(1)
    place = (lax.axis_index("z") * x_size + lax.axis_index("x")).astype(jnp.int32).reshape(1)
    smem = pl.BlockSpec(memory_space=pltpu.SMEM)
    vmem = pl.BlockSpec(memory_space=pltpu.VMEM)
    limit = pltpu.CompilerParams(vmem_limit_bytes=24 * 2**20)

    own_rows = pl.pallas_call(
        prepare_kernel,
        out_shape=pltpu.VMEM((8, rows, width + 128), bf16),
        in_specs=[smem] + [vmem] * 5,
        out_specs=vmem,
        compiler_params=limit,
        name="prepare",
    )(forget_bias, tokens, pre_gain.reshape(-1, 128), w_igate.T, w_fgate.T, gate_drift.T)
    with jax.named_scope("rows"):
        all_rows = lax.all_to_all(own_rows, ("c", "y"), split_axis=0, concat_axis=0, tiled=True)
    all_rows = near(all_rows.reshape(-1, width + 128))
    length = all_rows.shape[0]

    pair = jnp.stack(
        [
            jnp.concatenate(
                [
                    w_query[:, c * DK : (c + 1) * DK],
                    w_key[:, c * DK : (c + 1) * DK],
                    w_value[:, c * DV : (c + 1) * DV],
                    w_out[:, c * DV : (c + 1) * DV],
                ],
                axis=1,
            )
            for c in range(2)
        ]
    )
    with jax.named_scope("pair"):
        both = lax.all_gather(pair, "c", axis=0, tiled=False)
    mine = lax.dynamic_index_in_dim(both, core, axis=1, keepdims=False)
    mine = mine.reshape(-1, mine.shape[2])
    with jax.named_scope("along_z"):
        along_z = lax.all_gather(mine, "z", axis=0, tiled=True)
    cut = 2 * DK + DV

    def along_x(part):
        return lax.all_to_all(
            jnp.broadcast_to(part[None], (x_size,) + part.shape),
            "x",
            split_axis=0,
            concat_axis=0,
            tiled=True,
        )

    with jax.named_scope("w_in"):
        w_in = along_x(along_z[:, :cut])
    own_back = along_z[:, cut:]
    w_back = [own_back]
    for d in range(1, x_size):
        with jax.named_scope(f"w_back_{d}"):
            ring = [(k, (k + d) % x_size) for k in range(x_size)]
            w_back.append(lax.ppermute(own_back, "x", ring))

    pair_decay, aux, facts = pl.pallas_call(
        gates_kernel,
        out_shape=(
            pltpu.VMEM((length, length), f32),
            pltpu.VMEM((length, 128), f32),
            pltpu.VMEM((8, 128), f32),
        ),
        in_specs=[smem, vmem],
        out_specs=(vmem,) * 3,
        compiler_params=limit,
        name="gates",
    )(head, all_rows)
    query, key, value, message = pl.pallas_call(
        state_kernel,
        out_shape=(
            pltpu.VMEM((length, DK), bf16),
            pltpu.VMEM((length, DK), bf16),
            pltpu.VMEM((length, DV), bf16),
            pltpu.VMEM((peers * 8, DK), bf16),
        ),
        in_specs=[vmem] * 4,
        out_specs=(vmem,) * 4,
        scratch_shapes=[pltpu.VMEM((peers * 8, DK), f32)],
        compiler_params=limit,
        name="state",
    )(all_rows, near(w_in), aux, facts)
    with jax.named_scope("states_out"):
        arrived = lax.all_to_all(message, ROWS, split_axis=0, concat_axis=0, tiled=True)
    numer, denom = pl.pallas_call(
        intra_kernel,
        out_shape=(pltpu.VMEM((length, DV), f32), pltpu.VMEM((length, 128), f32)),
        in_specs=[vmem] * 4,
        out_specs=(vmem,) * 2,
        compiler_params=limit,
        name="intra",
    )(query, key, value, pair_decay)
    slices, entry = pl.pallas_call(
        prefix_kernel,
        out_shape=(pltpu.VMEM((DV, DK), f32), pltpu.VMEM((8, 128), f32)),
        in_specs=[smem, vmem],
        out_specs=(vmem,) * 2,
        scratch_shapes=[pltpu.VMEM((peers * 8, DK), f32)],
        compiler_params=limit,
        name="prefix",
    )(place, near(arrived))
    with jax.named_scope("states_back"):
        state = lax.all_to_all(slices, ROWS, split_axis=0, concat_axis=0, tiled=True)
    where = jnp.concatenate([head, lax.axis_index("x").astype(jnp.int32).reshape(1)])
    partial = pl.pallas_call(
        finish_kernel,
        out_shape=pltpu.VMEM((length, width), bf16),
        in_specs=[smem] + [vmem] * 11,
        out_specs=vmem,
        scratch_shapes=[pltpu.VMEM((x_size,) + own_back.shape, bf16)],
        compiler_params=limit,
        name="finish",
    )(
        where,
        query,
        numer,
        denom,
        aux,
        near(state),
        entry,
        head_gain.reshape(-1, 128),
        *[near(w) for w in w_back],
    )
    with jax.named_scope("heads"):
        halves = lax.all_to_all(
            partial.reshape(2, -1, width), "c", split_axis=0, concat_axis=0, tiled=True
        )
    joined = halves.astype(f32).sum(axis=0).astype(bf16)
    with jax.named_scope("owners"):
        pieces = lax.all_to_all(
            joined.reshape(-1, rows, width), "y", split_axis=0, concat_axis=0, tiled=True
        )
    return pieces.astype(f32).sum(axis=0).astype(bf16)


def solution(mesh):
    split = Mesh(mesh.devices.reshape(16, 4, 2, mesh.shape["tp"]), ("z", "x", "c", "y"))
    return jax.shard_map(
        on_device,
        mesh=split,
        in_specs=(
            P(SP_TP, None),
            P(),
            P(SP, "y"),
            P(SP, "y"),
            P(SP, "y"),
            P(),
            P(),
            P(),
            P(SP, None),
            P(),
            P(SP, "y"),
        ),
        out_specs=P(SP_TP, None),
        check_vma=False,
    )
```

time: 177 us -> 152 us (0.86)
  starting transfers between devices: 16.6 us -> 38.1 us
  waiting for transfers between devices: 50.6 us -> 35.3 us
  between operations: 13.6 us -> 0.2 us
  blocking collectives: 68.2 us -> 57.2 us
  Pallas kernels: 12.6 us -> 8.35 us
  local copies, waits for them, and re-layouts: 12.9 us -> 11 us
    all_to_all x1, waiting for transfers between devices: 14.5 us -> 0.01 us  [on_device(): lax.all_to_all(slices, ROWS, split_axis=0, concat_axis=0, tiled=True)]
    all_to_all x2, blocking collectives: 39.9 us -> 26 us  [the longest x1 14.6 us: on_device(): lax.all_to_all(partial.reshape(2, -1, width), 'c', split_axis=0, concat_a...]
    all_to_all x1 -> x2, starting transfers between devices: 4.01 us -> 14.4 us  [the longest x1 10.3 us: on_device(): lax.all_to_all(own_rows, ('c', 'y'), split_axis=0, concat_axis=0, tiled=T...]
    ppermute x0 -> x3, starting transfers between devices: none -> 10.2 us  [on_device(): w_back.append(lax.ppermute(own_back, 'x', ring))]
    pallas_call x4 -> x6, Pallas kernels: 12.6 us -> 8.35 us  [the longest x1 2.24 us: on_device(): pl.pallas_call(prepare_kernel, out_shape=pltpu.VMEM((8, rows, width + 128...]
    unnamed x18 -> x32, local copies, waits for them, and re-layouts: 4.77 us -> 8.46 us
    concatenate x2 -> x0, local copies, waits for them, and re-layouts: 2.54 us -> none  [the longest x1 2.46 us: on_device(): jnp.concatenate([w_igate, w_fgate] * 3 + [jnp.zeros((width, 80), bf16)],...]
    all_to_all x1, waiting for transfers between devices: 17.5 us -> 15 us  [on_device(): lax.all_to_all(message, ROWS, split_axis=0, concat_axis=0, tiled=True)]
  transfers between devices with their start and end apart: 5 -> 7, of which waited for: 3 -> 4; matrix products, arithmetic and copies ran while one was open for 2% -> 1% of each run, Pallas kernels for 4% -> 1%
where the time goes in v2:
time: 152 us; the launch traced here: 151 us
  blocking collectives  57.2 us (38%)
  starting transfers between devices  38.1 us (25%)
  waiting for transfers between devices  35.3 us (23%)
  local copies, waits for them, and re-layouts  11 us (7%)
  Pallas kernels  8.35 us (5%)
    all_gather x1, blocking collectives, on_device(): along_z = lax.all_gather(mine, 'z', axis=0, tiled=True)  29.3 us
    all_to_all x1, waiting for transfers between devices, along_x(): lax.all_to_all(jnp.broadcast_to(part[None], (x_size,) + part.shape), 'x',...  18 us
    all_to_all x1, waiting for transfers between devices, on_device(): lax.all_to_all(message, ROWS, split_axis=0, concat_axis=0, tiled=True)  15 us
    all_to_all x1, blocking collectives, on_device(): lax.all_to_all(partial.reshape(2, -1, width), 'c', split_axis=0, concat_a...  14.6 us
    all_to_all x1, blocking collectives, on_device(): lax.all_to_all(joined.reshape(-1, rows, width), 'y', split_axis=0, concat...  11.5 us
    all_to_all x1, starting transfers between devices, on_device(): lax.all_to_all(own_rows, ('c', 'y'), split_axis=0, concat_axis=0, tiled=T...  10.3 us
    ppermute x3, starting transfers between devices, on_device(): w_back.append(lax.ppermute(own_back, 'x', ring))  10.2 us
    all_to_all x1, starting transfers between devices, on_device(): lax.all_to_all(message, ROWS, split_axis=0, concat_axis=0, tiled=True)  8.91 us
  transfers between devices with their start and end apart: 7, of which 4 were waited for; matrix products, arithmetic and copies ran while one was open for 1% of the time, Pallas kernels for 1%

profile of v2, /device:TPU:1, one launch (start us, length us, event | category | flops | bytes accessed | tf_op | source)
XLA Modules:
  0.0 151.3 jit_solution(9443332414163841805)
XLA Ops:
  0.0 0.9 copy-done.2
  0.9 0.8 copy-done.5
  1.7 0.8 copy-done.6
  2.4 0.7 copy-done.7
  3.1 0.7 copy-done.8
  3.8 0.7 copy-done.10
  4.5 2.2 %prepare.1 = bf16[8,32,2176]{2,1,0:T(8,128)(2,1)} custom-call(f32[8]{0:T(128)S(1)} %copy-done.10, bf16[32,2048]{1,0:T(8,128)(2,1)S(1)} %copy-done.2, bf16[16,128]{1,0:T(8,128)(2,1)S(1)} %bitcast.30, bf16[8,2048]{1,0:T(8,128)(2,1)S(1)} %bitcast.28, bf16[8,2048]{1,0:T(8,128)(2,1)S(1)} %bitcast.29, f32[8,128]{1,0:T(8,128)S(1)} %bitcast.31), custom_call_target="tpu_custom_call" | custom-call | tf_op jit(solution)/shard_map/prepare/pallas_call | solution.py:288
  6.7 10.3 %all-to-all-start = ((bf16[8,32,2176]{2,1,0:T(8,128)(2,1)}), bf16[8,32,2176]{2,1,0:T(8,128)(2,1)S(1)}, u32[]{:S(2)}, u32[]{:S(2)}) async-start(bf16[8,32,2176]{2,1,0:T(8,128)(2,1)} %prepare.1), calls=%async_computation | async-start | bytes 2228224 | tf_op jit(solution)/shard_map/rows/all_to_all | solution.py:297
  17.1 1.9 %all-gather = bf16[4,16,768]{2,1,0:T(8,128)(2,1)S(1)} all-gather(bf16[2,16,768]{2,1,0:T(8,128)(2,1)S(1)} %pad_maximum_fusion), channel_id=2, replica_groups=mesh['z'=16,'x'=4,'c'=2,'y'=4] {'c'}, dimensions={0}, use_global_device_ids=true | all-gather | bytes 147456 | tf_op jit(solution)/shard_map/pair/all_gather | solution.py:316
  19.0 29.3 %all_gather.11 = bf16[512,768]{1,0:T(8,128)(2,1)S(1)} all-gather(bf16[32,768]{1,0:T(8,128)(2,1)S(1)} %bitcast.35), channel_id=1, replica_groups=mesh['z'=16,'x'=4,'c'=2,'y'=4] {'z'}, dimensions={0}, use_global_device_ids=true | all-gather | bytes 835584 | tf_op jit(solution)/shard_map/along_z/all_gather | solution.py:320
  48.3 0.9 copy-done.11
  49.2 1.5 %broadcast_in_dim.2 = bf16[4,512,512]{2,1,0:T(8,128)(2,1)} broadcast(bf16[512,512]{1,0:T(8,128)(2,1)S(1)} %slice.40), dimensions={1,2} | broadcast | bytes 2621440 | tf_op jit(solution)/shard_map/w_in/broadcast_in_dim | solution.py:325
  50.7 4.1 %all-to-all-start.1 = ((bf16[4,512,512]{2,1,0:T(8,128)(2,1)}), bf16[4,512,512]{2,1,0:T(8,128)(2,1)S(1)}, u32[]{:S(2)}, u32[]{:S(2)}) async-start(bf16[4,512,512]{2,1,0:T(8,128)(2,1)} %broadcast_in_dim.2), calls=%async_computation.1 | async-start | bytes 4194304 | tf_op jit(solution)/shard_map/w_in/all_to_all | solution.py:324
  55.4 0.7 copy-done
  56.1 18.0 %all-to-all-done.1.w_ref = bf16[4,512,512]{2,1,0:T(8,128)(2,1)S(1)} async-done(((bf16[4,512,512]{2,1,0:T(8,128)(2,1)}), bf16[4,512,512]{2,1,0:T(8,128)(2,1)S(1)}, u32[]{:S(2)}, u32[]{:S(2)}) %all-to-all-start.1) | async-done | bytes 2097184 | tf_op jit(solution)/shard_map/w_in/all_to_all | solution.py:324
  74.1 2.2 %state.1 = (bf16[256,128]{1,0:T(8,128)(2,1)S(1)}, bf16[256,128]{1,0:T(8,128)(2,1)S(1)}, bf16[256,256]{1,0:T(8,128)(2,1)S(1)}, bf16[512,128]{1,0:T(8,128)(2,1)}) custom-call(bf16[256,2176]{1,0:T(8,128)(2,1)S(1)} %bitcast.24, bf16[4,512,512]{2,1,0:T(8,128)(2,1)S(1)} %all-to-all-done.1.w_ref, f32[256,128]{1,0:T(8,128)S(1)} %get-tuple-element.16.aux_ref, ...), custom_call_target="tpu_custom_call" | custom-call | tf_op jit(solution)/shard_map/state/pallas_call | solution.py:353
  76.3 0.6 copy-done.3
  76.9 8.9 %all-to-all-start.2 = ((bf16[64,8,128]{2,1,0:T(8,128)(2,1)}), bf16[64,8,128]{2,1,0:T(8,128)(2,1)S(1)}, u32[]{:S(2)}, u32[]{:S(2)}) async-start(bf16[64,8,128]{2,1,0:T(8,128)(2,1)} %bitcast.12), calls=%async_computation.2 | async-start | bytes 262144 | tf_op jit(solution)/shard_map/states_out/all_to_all | solution.py:368
  85.9 15.0 %all-to-all-done.2 = bf16[64,8,128]{2,1,0:T(8,128)(2,1)S(1)} async-done(((bf16[64,8,128]{2,1,0:T(8,128)(2,1)}), bf16[64,8,128]{2,1,0:T(8,128)(2,1)S(1)}, u32[]{:S(2)}, u32[]{:S(2)}) %all-to-all-start.2) | async-done | bytes 131104 | tf_op jit(solution)/shard_map/states_out/all_to_all | solution.py:368
  100.8 1.2 prefix.1
  102.1 4.6 %all-to-all-start.3 = ((f32[64,4,128]{2,1,0:T(4,128)}), f32[64,4,128]{2,1,0:T(4,128)S(1)}, u32[]{:S(2)}, u32[]{:S(2)}) async-start(f32[64,4,128]{2,1,0:T(4,128)} %bitcast.14), calls=%async_computation.3 | async-start | bytes 262144 | tf_op jit(solution)/shard_map/states_back/all_to_all | solution.py:387
  106.7 1.0 slice.41.w_0_ref
  107.7 2.8 %collective-permute-start = (bf16[512,256]{1,0:T(8,128)(2,1)S(1)}, bf16[512,256]{1,0:T(8,128)(2,1)S(1)}, u32[]{:S(2)}, u32[]{:S(2)}) collective-permute-start(bf16[512,256]{1,0:T(8,128)(2,1)S(1)} %slice.41.w_0_ref), channel_id=1, source_target_pairs={{0,8},{8,16},{16,24},{24,0},{1,9},{9,17},{17,25},{25,1},{2,10},{10... | collective-permute-start | bytes 786440 | tf_op jit(solution)/shard_map/w_back_1/ppermute | solution.py:339
  110.5 4.3 %collective-permute-start.1 = (bf16[512,256]{1,0:T(8,128)(2,1)S(1)}, bf16[512,256]{1,0:T(8,128)(2,1)S(1)}, u32[]{:S(2)}, u32[]{:S(2)}) collective-permute-start(bf16[512,256]{1,0:T(8,128)(2,1)S(1)} %slice.41.w_0_ref), channel_id=1, source_target_pairs={{0,16},{8,24},{16,0},{24,8},{1,17},{9,25},{17,1},{25,9},{2,18},{10... | collective-permute-start | bytes 786440 | tf_op jit(solution)/shard_map/w_back_2/ppermute | solution.py:339
  114.8 3.1 %collective-permute-start.2 = (bf16[512,256]{1,0:T(8,128)(2,1)S(1)}, bf16[512,256]{1,0:T(8,128)(2,1)S(1)}, u32[]{:S(2)}, u32[]{:S(2)}) collective-permute-start(bf16[512,256]{1,0:T(8,128)(2,1)S(1)} %slice.41.w_0_ref), channel_id=1, source_target_pairs={{0,24},{8,0},{16,8},{24,16},{1,25},{9,1},{17,9},{25,17},{2,26},{10... | collective-permute-start | bytes 786440 | tf_op jit(solution)/shard_map/w_back_3/ppermute | solution.py:339
  118.0 0.9 copy-done.1
  118.9 0.8 copy-done.4
  120.2 2.2 %collective-permute-done.2.w_3_ref = bf16[512,256]{1,0:T(8,128)(2,1)S(1)} collective-permute-done((bf16[512,256]{1,0:T(8,128)(2,1)S(1)}, bf16[512,256]{1,0:T(8,128)(2,1)S(1)}, u32[]{:S(2)}, u32[]{:S(2)}) %collective-permute-start.2) | collective-permute-done | bytes 262176 | tf_op jit(solution)/shard_map/w_back_3/ppermute | solution.py:339
  122.4 1.8 %finish.1 = bf16[256,2048]{1,0:T(8,128)(2,1)S(1)} custom-call(s32[2]{0:T(128)S(1)} %pad_add_fusion.head_ref, bf16[256,128]{1,0:T(8,128)(2,1)S(1)} %get-tuple-element.18.query_ref, f32[256,256]{1,0:T(8,128)S(1)} %get-tuple-element.22.numer_ref, f32[256,128]{1,0:T(8,128)S(1)} %get-tuple-element.23.denom_ref, f32[256,128]{1,0:T(8,128)S(1)} %get-tuple-element.16.aux_ref, ...), custom_call_target="tpu_custom_call" | custom-call | tf_op jit(solution)/shard_map/finish/pallas_call | solution.py:389
  124.2 14.6 %all_to_all.42 = bf16[2,128,2048]{2,1,0:T(8,128)(2,1)S(1)} all-to-all(bf16[2,128,2048]{2,1,0:T(8,128)(2,1)S(1)} %bitcast.25), channel_id=1, replica_groups=mesh['z'=16,'x'=4,'c'=2,'y'=4] {'c'}, dimensions={0} | all-to-all | bytes 2097152 | tf_op jit(solution)/shard_map/heads/all_to_all | solution.py:409
  139.1 11.5 %all_to_all.43 = bf16[4,32,2048]{2,1,0:T(8,128)(2,1)S(1)} all-to-all(bf16[4,32,2048]{2,1,0:T(8,128)(2,1)S(1)} %bitcast.33), channel_id=1, replica_groups=mesh['z'=16,'x'=4,'c'=2,'y'=4] {'y'}, dimensions={0} | all-to-all | bytes 1048576 | tf_op jit(solution)/shard_map/owners/all_to_all | solution.py:414
  150.6 0.7 reduce_sum.25
  (37 shorter events, 1.5 us)
Async XLA Ops:
  0.0 0.9 copy-start.2
  0.9 0.8 copy-start.5
  1.7 0.8 copy-start.6
  2.4 0.7 copy-start.7
  3.1 0.7 copy-start.8
  3.8 0.7 copy-start.10
  4.5 12.6 %copy-start.12 = (bf16[16,512]{1,0:T(8,128)(2,1)S(1)}, bf16[16,512]{1,0:T(8,128)(2,1)}, u32[]{:S(2)}) copy-start(bf16[16,512]{1,0:T(8,128)(2,1)} %param.15) | copy-start | bytes 49156
  4.5 12.6 %copy-start.14 = (bf16[16,256]{1,0:T(8,128)(2,1)S(1)}, bf16[16,256]{1,0:T(8,128)(2,1)}, u32[]{:S(2)}) copy-start(bf16[16,256]{1,0:T(8,128)(2,1)} %param.13) | copy-start | bytes 24580
  4.5 12.6 %copy-start.15 = (bf16[16,256]{1,0:T(8,128)(2,1)S(1)}, bf16[16,256]{1,0:T(8,128)(2,1)}, u32[]{:S(2)}) copy-start(bf16[16,256]{1,0:T(8,128)(2,1)} %param.14) | copy-start | bytes 24580
  4.5 12.6 %copy-start.13 = (bf16[16,512]{1,0:T(8,128)(2,1)S(1)}, bf16[16,512]{1,0:T(8,128)(2,1)}, u32[]{:S(2)}) copy-start(bf16[16,512]{1,0:T(8,128)(2,1)} %param.21) | copy-start | bytes 49156
  6.7 42.5 %all-to-all-start = ((bf16[8,32,2176]{2,1,0:T(8,128)(2,1)}), bf16[8,32,2176]{2,1,0:T(8,128)(2,1)S(1)}, u32[]{:S(2)}, u32[]{:S(2)}) async-start(bf16[8,32,2176]{2,1,0:T(8,128)(2,1)} %prepare.1), calls=%async_computation | async-start | bytes 2228224 | tf_op jit(solution)/shard_map/rows/all_to_all | solution.py:297
  48.3 0.9 copy-start.11
  50.7 23.4 %all-to-all-start.1 = ((bf16[4,512,512]{2,1,0:T(8,128)(2,1)}), bf16[4,512,512]{2,1,0:T(8,128)(2,1)S(1)}, u32[]{:S(2)}, u32[]{:S(2)}) async-start(bf16[4,512,512]{2,1,0:T(8,128)(2,1)} %broadcast_in_dim.2), calls=%async_computation.1 | async-start | bytes 4194304 | tf_op jit(solution)/shard_map/w_in/all_to_all | solution.py:324
  55.4 0.7 copy-start
  74.1 48.3 %copy-start.9 = (bf16[2048]{0:T(1024)(128)(2,1)S(1)}, bf16[2048]{0:T(1024)(128)(2,1)}, u32[]{:S(2)}) copy-start(bf16[2048]{0:T(1024)(128)(2,1)} %param.20) | copy-start | bytes 12292
  76.3 0.6 copy-start.3
  76.9 23.9 %all-to-all-start.2 = ((bf16[64,8,128]{2,1,0:T(8,128)(2,1)}), bf16[64,8,128]{2,1,0:T(8,128)(2,1)S(1)}, u32[]{:S(2)}, u32[]{:S(2)}) async-start(bf16[64,8,128]{2,1,0:T(8,128)(2,1)} %bitcast.12), calls=%async_computation.2 | async-start | bytes 262144 | tf_op jit(solution)/shard_map/states_out/all_to_all | solution.py:368
  102.1 20.3 %all-to-all-start.3 = ((f32[64,4,128]{2,1,0:T(4,128)}), f32[64,4,128]{2,1,0:T(4,128)S(1)}, u32[]{:S(2)}, u32[]{:S(2)}) async-start(f32[64,4,128]{2,1,0:T(4,128)} %bitcast.14), calls=%async_computation.3 | async-start | bytes 262144 | tf_op jit(solution)/shard_map/states_back/all_to_all | solution.py:387
  107.7 12.4 %collective-permute-start = (bf16[512,256]{1,0:T(8,128)(2,1)S(1)}, bf16[512,256]{1,0:T(8,128)(2,1)S(1)}, u32[]{:S(2)}, u32[]{:S(2)}) collective-permute-start(bf16[512,256]{1,0:T(8,128)(2,1)S(1)} %slice.41.w_0_ref), channel_id=1, source_target_pairs={{0,8},{8,16},{16,24},{24,0},{1,9},{9,17},{17,25},{25,1},{2,10},{10... | collective-permute-start | bytes 786440 | tf_op jit(solution)/shard_map/w_back_1/ppermute | solution.py:339
  110.5 9.7 %collective-permute-start.1 = (bf16[512,256]{1,0:T(8,128)(2,1)S(1)}, bf16[512,256]{1,0:T(8,128)(2,1)S(1)}, u32[]{:S(2)}, u32[]{:S(2)}) collective-permute-start(bf16[512,256]{1,0:T(8,128)(2,1)S(1)} %slice.41.w_0_ref), channel_id=1, source_target_pairs={{0,16},{8,24},{16,0},{24,8},{1,17},{9,25},{17,1},{25,9},{2,18},{10... | collective-permute-start | bytes 786440 | tf_op jit(solution)/shard_map/w_back_2/ppermute | solution.py:339
  114.8 7.6 %collective-permute-start.2 = (bf16[512,256]{1,0:T(8,128)(2,1)S(1)}, bf16[512,256]{1,0:T(8,128)(2,1)S(1)}, u32[]{:S(2)}, u32[]{:S(2)}) collective-permute-start(bf16[512,256]{1,0:T(8,128)(2,1)S(1)} %slice.41.w_0_ref), channel_id=1, source_target_pairs={{0,24},{8,0},{16,8},{24,16},{1,25},{9,1},{17,9},{25,17},{2,26},{10... | collective-permute-start | bytes 786440 | tf_op jit(solution)/shard_map/w_back_3/ppermute | solution.py:339
  118.0 1.0 copy-start.1
  118.9 0.8 copy-start.4

commit v3 on v2

--- a/solution.py
+++ b/solution.py
@@ -76,7 +76,13 @@
         out_ref[k, :, width:] = piece
 
 
-def gates_kernel(head_ref, rows_ref, pair_ref, aux_ref, facts_ref):
+def gates_kernel(
+    head_ref, rows_ref, along_ref, pair_ref, aux_ref, facts_ref, copies_ref, own_back_ref
+):
+    cut = copies_ref.shape[2]
+    for k in range(copies_ref.shape[0]):
+        copies_ref[k] = along_ref[:, :cut]
+    own_back_ref[...] = along_ref[:, cut:]
     head = head_ref[0]
     gates = rows_ref[:, -128:].astype(f32)
     length = gates.shape[0]
@@ -118,8 +124,20 @@
 
 
 def state_kernel(
-    rows_ref, w_ref, aux_ref, facts_ref, query_ref, key_ref, value_ref, message_ref, buffer_ref
+    rows_ref,
+    w_ref,
+    aux_ref,
+    facts_ref,
+    pair_ref,
+    own_back_ref,
+    query_ref,
+    numer_ref,
+    denom_ref,
+    message_ref,
+    passed_ref,
+    buffer_ref,
 ):
+    passed_ref[...] = own_back_ref[...]
     length, width = rows_ref.shape[0], rows_ref.shape[1] - 128
     x_size = w_ref.shape[0]
     run = 32
@@ -133,11 +151,10 @@
             jnp.concatenate(parts, axis=0),
             preferred_element_type=f32,
         )
-    query_ref[...] = total[:, :DK].astype(bf16)
+    query = total[:, :DK].astype(bf16)
+    query_ref[...] = query
     key = (total[:, DK : 2 * DK] * (DK**-0.5)).astype(bf16)
     value = total[:, 2 * DK :].astype(bf16)
-    key_ref[...] = key
-    value_ref[...] = value
     scaled_key = key.astype(f32) * column_of(aux_ref[...], 3)
     state = jnp.dot(value.astype(f32).T, scaled_key, precision=highest, preferred_element_type=f32)
     vector = jnp.sum(scaled_key, axis=0, keepdims=True)
@@ -149,19 +166,18 @@
     for r in (6, 7):
         buffer_ref[pl.ds(r, peers, stride=8), :] = jnp.zeros((peers, DK), f32)
     message_ref[...] = buffer_ref[...].astype(bf16)
-
-
-def intra_kernel(query_ref, key_ref, value_ref, pair_ref, numer_ref, denom_ref):
-    scores = lax.dot_general(
-        query_ref[...], key_ref[...], (((1,), (1,)), ((), ())), preferred_element_type=f32
-    )
+    scores = lax.dot_general(query, key, (((1,), (1,)), ((), ())), preferred_element_type=f32)
     weights = scores * pair_ref[...]
-    numer_ref[...] = jnp.dot(weights.astype(bf16), value_ref[...], preferred_element_type=f32)
+    numer_ref[...] = jnp.dot(weights.astype(bf16), value, preferred_element_type=f32)
     denom = jnp.sum(weights, axis=1, keepdims=True)
     denom_ref[...] = jnp.broadcast_to(denom, denom_ref.shape)
 
 
-def prefix_kernel(place_ref, arrived_ref, out_ref, entry_ref, buffer_ref):
+def prefix_kernel(
+    place_ref, arrived_ref, own_back_ref, over_two_ref, out_ref, entry_ref, double_ref, buffer_ref
+):
+    double_ref[0] = own_back_ref[...]
+    double_ref[1] = over_two_ref[...]
     place = place_ref[0]
     buffer_ref[...] = arrived_ref[...].astype(f32)
     peers = buffer_ref.shape[0] // 8
@@ -204,17 +220,16 @@
     state_ref,
     entry_ref,
     gain_ref,
-    w_0_ref,
-    w_1_ref,
-    w_2_ref,
-    w_3_ref,
+    double_ref,
+    next_ref,
     out_ref,
     w_ref,
 ):
     head = head_ref[0]
     my_x = head_ref[1]
-    for d, piece_ref in enumerate((w_0_ref, w_1_ref, w_2_ref, w_3_ref)):
-        w_ref[(my_x + 4 - d) % 4] = piece_ref[...]
+    for k in range(2):
+        w_ref[(my_x + 2 * k) % 4] = double_ref[k]
+        w_ref[(my_x + 3 + 2 * k) % 4] = next_ref[k]
     peers = 64
     count = state_ref.shape[0] // peers
     state = jnp.concatenate(
@@ -290,7 +305,6 @@
         out_shape=pltpu.VMEM((8, rows, width + 128), bf16),
         in_specs=[smem] + [vmem] * 5,
         out_specs=vmem,
-        compiler_params=limit,
         name="prepare",
     )(forget_bias, tokens, pre_gain.reshape(-1, 128), w_igate.T, w_fgate.T, gate_drift.T)
     with jax.named_scope("rows"):
@@ -320,76 +334,67 @@
         along_z = lax.all_gather(mine, "z", axis=0, tiled=True)
     cut = 2 * DK + DV
 
-    def along_x(part):
-        return lax.all_to_all(
-            jnp.broadcast_to(part[None], (x_size,) + part.shape),
-            "x",
-            split_axis=0,
-            concat_axis=0,
-            tiled=True,
-        )
-
-    with jax.named_scope("w_in"):
-        w_in = along_x(along_z[:, :cut])
-    own_back = along_z[:, cut:]
-    w_back = [own_back]
-    for d in range(1, x_size):
-        with jax.named_scope(f"w_back_{d}"):
-            ring = [(k, (k + d) % x_size) for k in range(x_size)]
-            w_back.append(lax.ppermute(own_back, "x", ring))
-
-    pair_decay, aux, facts = pl.pallas_call(
+    pair_decay, aux, facts, copies, own_back = pl.pallas_call(
         gates_kernel,
         out_shape=(
             pltpu.VMEM((length, length), f32),
             pltpu.VMEM((length, 128), f32),
             pltpu.VMEM((8, 128), f32),
+            pltpu.VMEM((x_size, along_z.shape[0], cut), bf16),
+            pltpu.VMEM((along_z.shape[0], along_z.shape[1] - cut), bf16),
         ),
-        in_specs=[smem, vmem],
-        out_specs=(vmem,) * 3,
+        in_specs=[smem, vmem, vmem],
+        out_specs=(vmem,) * 5,
         compiler_params=limit,
         name="gates",
-    )(head, all_rows)
-    query, key, value, message = pl.pallas_call(
+    )(head, all_rows, near(along_z))
+    with jax.named_scope("w_in"):
+        w_in = lax.all_to_all(copies, "x", split_axis=0, concat_axis=0, tiled=True)
+    query, numer, denom, message, own_back = pl.pallas_call(
         state_kernel,
         out_shape=(
             pltpu.VMEM((length, DK), bf16),
-            pltpu.VMEM((length, DK), bf16),
-            pltpu.VMEM((length, DV), bf16),
+            pltpu.VMEM((length, DV), f32),
+            pltpu.VMEM((length, 128), f32),
             pltpu.VMEM((peers * 8, DK), bf16),
+            pltpu.VMEM(own_back.shape, bf16),
         ),
-        in_specs=[vmem] * 4,
-        out_specs=(vmem,) * 4,
+        in_specs=[vmem] * 6,
+        out_specs=(vmem,) * 5,
         scratch_shapes=[pltpu.VMEM((peers * 8, DK), f32)],
         compiler_params=limit,
         name="state",
-    )(all_rows, near(w_in), aux, facts)
+    )(all_rows, near(w_in), aux, facts, pair_decay, own_back)
     with jax.named_scope("states_out"):
         arrived = lax.all_to_all(message, ROWS, split_axis=0, concat_axis=0, tiled=True)
-    numer, denom = pl.pallas_call(
-        intra_kernel,
-        out_shape=(pltpu.VMEM((length, DV), f32), pltpu.VMEM((length, 128), f32)),
-        in_specs=[vmem] * 4,
-        out_specs=(vmem,) * 2,
-        compiler_params=limit,
-        name="intra",
-    )(query, key, value, pair_decay)
-    slices, entry = pl.pallas_call(
+
+    def ring(d):
+        return [(k, (k + d) % x_size) for k in range(x_size)]
+
+    with jax.named_scope("over_two"):
+        over_two = lax.ppermute(own_back, "x", ring(2))
+    slices, entry, double = pl.pallas_call(
         prefix_kernel,
-        out_shape=(pltpu.VMEM((DV, DK), f32), pltpu.VMEM((8, 128), f32)),
-        in_specs=[smem, vmem],
-        out_specs=(vmem,) * 2,
+        out_shape=(
+            pltpu.VMEM((DV, DK), f32),
+            pltpu.VMEM((8, 128), f32),
+            pltpu.VMEM((2,) + own_back.shape, bf16),
+        ),
+        in_specs=[smem, vmem, vmem, vmem],
+        out_specs=(vmem,) * 3,
         scratch_shapes=[pltpu.VMEM((peers * 8, DK), f32)],
         compiler_params=limit,
         name="prefix",
-    )(place, near(arrived))
+    )(place, near(arrived), own_back, near(over_two))
     with jax.named_scope("states_back"):
         state = lax.all_to_all(slices, ROWS, split_axis=0, concat_axis=0, tiled=True)
+    with jax.named_scope("over_one"):
+        following = lax.ppermute(double, "x", ring(1))
     where = jnp.concatenate([head, lax.axis_index("x").astype(jnp.int32).reshape(1)])
     partial = pl.pallas_call(
         finish_kernel,
         out_shape=pltpu.VMEM((length, width), bf16),
-        in_specs=[smem] + [vmem] * 11,
+        in_specs=[smem] + [vmem] * 9,
         out_specs=vmem,
         scratch_shapes=[pltpu.VMEM((x_size,) + own_back.shape, bf16)],
         compiler_params=limit,
@@ -403,7 +408,8 @@
         near(state),
         entry,
         head_gain.reshape(-1, 128),
-        *[near(w) for w in w_back],
+        double,
+        near(following),
     )
     with jax.named_scope("heads"):
         halves = lax.all_to_all(

time: 152 us -> 153 us (level)
  blocking collectives: 57.2 us -> 82.6 us
  local copies, waits for them, and re-layouts: 11 us -> 0.04 us
  waiting for transfers between devices: 35.3 us -> 25.5 us
  starting transfers between devices: 38.1 us -> 34.5 us
    all_to_all x0 -> x1, blocking collectives: none -> 23.5 us  [on_device(): w_in = lax.all_to_all(copies, 'x', split_axis=0, concat_axis=0, tiled=True)]
    all_to_all x1 -> x0, waiting for transfers between devices: 18 us -> none  [along_x(): lax.all_to_all(jnp.broadcast_to(part[None], (x_size,) + part.shape), 'x',...]
    all_to_all x1, waiting for transfers between devices: 0.01 us -> 14.9 us  [on_device(): lax.all_to_all(slices, ROWS, split_axis=0, concat_axis=0, tiled=True)]
    all_to_all x1, waiting for transfers between devices: 15 us -> 6.09 us  [on_device(): lax.all_to_all(message, ROWS, split_axis=0, concat_axis=0, tiled=True)]
    unnamed x32 -> x10, local copies, waits for them, and re-layouts: 8.46 us -> 0.02 us
    all_to_all x1, starting transfers between devices: 4.62 us -> 9.09 us  [on_device(): lax.all_to_all(slices, ROWS, split_axis=0, concat_axis=0, tiled=True)]
    all_to_all x1 -> x0, starting transfers between devices: 4.06 us -> none  [along_x(): lax.all_to_all(jnp.broadcast_to(part[None], (x_size,) + part.shape), 'x',...]
    ppermute x3 -> x2, starting transfers between devices: 10.2 us -> 6.58 us  [the longest x1 4.42 us: on_device(): over_two = lax.ppermute(own_back, 'x', ring(2))]
  transfers between devices with their start and end apart: 7 -> 5, of which waited for: 4 -> 3; matrix products, arithmetic and copies ran while one was open for 1% -> 0% of each run, Pallas kernels for 1% -> 0%
where the time goes in v3:
time: 153 us; the launch traced here: 152 us
  blocking collectives  82.6 us (54%)
  starting transfers between devices  34.5 us (23%)
  waiting for transfers between devices  25.5 us (17%)
  Pallas kernels  8.47 us (6%)
    all_gather x1, blocking collectives, on_device(): along_z = lax.all_gather(mine, 'z', axis=0, tiled=True)  29.3 us
    all_to_all x1, blocking collectives, on_device(): w_in = lax.all_to_all(copies, 'x', split_axis=0, concat_axis=0, tiled=True)  23.5 us
    all_to_all x1, blocking collectives, on_device(): lax.all_to_all(partial.reshape(2, -1, width), 'c', split_axis=0, concat_a...  16.3 us
    all_to_all x1, waiting for transfers between devices, on_device(): lax.all_to_all(slices, ROWS, split_axis=0, concat_axis=0, tiled=True)  14.9 us
    all_to_all x1, blocking collectives, on_device(): lax.all_to_all(joined.reshape(-1, rows, width), 'y', split_axis=0, concat...  11.7 us
    all_to_all x1, starting transfers between devices, on_device(): lax.all_to_all(own_rows, ('c', 'y'), split_axis=0, concat_axis=0, tiled=T...  10.3 us
    all_to_all x1, starting transfers between devices, on_device(): lax.all_to_all(slices, ROWS, split_axis=0, concat_axis=0, tiled=True)  9.09 us
    all_to_all x1, starting transfers between devices, on_device(): lax.all_to_all(message, ROWS, split_axis=0, concat_axis=0, tiled=True)  8.5 us
  transfers between devices with their start and end apart: 5, of which 3 were waited for; matrix products, arithmetic and copies ran while one was open for 0% of the time, Pallas kernels for 0%

profile of v3, /device:TPU:1, one launch (start us, length us, event | category | flops | bytes accessed | tf_op | source)
XLA Modules:
  0.0 152.4 jit_solution(6803896874544743086)
XLA Ops:
  0.0 0.0 copy-start.3
  0.0 0.0 copy-start.1
  0.0 0.0 copy-start.4
  0.0 0.0 copy-start.2
  0.0 2.7 %prepare.1 = bf16[8,32,2176]{2,1,0:T(8,128)(2,1)} custom-call(f32[8]{0:T(128)} %bias_ref.1, bf16[32,2048]{1,0:T(8,128)(2,1)} %tokens_ref.1, bf16[16,128]{1,0:T(8,128)(2,1)} %bitcast.34, bf16[8,2048]{1,0:T(8,128)(2,1)} %bitcast.32, bf16[8,2048]{1,0:T(8,128)(2,1)} %bitcast.33, f32[8,128]{1,0:T(8,128)} %bitcast.35), custom_call_target="tpu_custom_call" | custom-call | tf_op jit(solution)/shard_map/prepare/pallas_call | solution.py:303
  2.7 10.3 %all-to-all-start = ((bf16[8,32,2176]{2,1,0:T(8,128)(2,1)}), bf16[8,32,2176]{2,1,0:T(8,128)(2,1)S(1)}, u32[]{:S(2)}, u32[]{:S(2)}) async-start(bf16[8,32,2176]{2,1,0:T(8,128)(2,1)} %prepare.1), calls=%async_computation | async-start | bytes 2228224 | tf_op jit(solution)/shard_map/rows/all_to_all | solution.py:311
  13.0 0.0 copy-done.3
  13.0 0.0 copy-done.1
  13.0 0.0 copy-done.4
  13.1 0.0 copy-done.2
  13.1 1.9 %all-gather = bf16[4,16,768]{2,1,0:T(8,128)(2,1)S(1)} all-gather(bf16[2,16,768]{2,1,0:T(8,128)(2,1)S(1)} %pad_maximum_fusion), channel_id=2, replica_groups=mesh['z'=16,'x'=4,'c'=2,'y'=4] {'c'}, dimensions={0}, use_global_device_ids=true | all-gather | bytes 147456 | tf_op jit(solution)/shard_map/pair/all_gather | solution.py:330
  15.0 29.3 %all_gather.11.along_ref = bf16[512,768]{1,0:T(8,128)(2,1)S(1)} all-gather(bf16[32,768]{1,0:T(8,128)(2,1)S(1)} %bitcast.31), channel_id=1, replica_groups=mesh['z'=16,'x'=4,'c'=2,'y'=4] {'z'}, dimensions={0}, use_global_device_ids=true | all-gather | bytes 835584 | tf_op jit(solution)/shard_map/along_z/all_gather | solution.py:334
  44.3 0.0 all-to-all-done
  44.3 0.6 gates.1
  44.9 23.5 %all_to_all.42.w_ref = bf16[4,512,512]{2,1,0:T(8,128)(2,1)S(1)} all-to-all(bf16[4,512,512]{2,1,0:T(8,128)(2,1)S(1)} %get-tuple-element.18), channel_id=1, replica_groups=mesh['z'=16,'x'=4,'c'=2,'y'=4] {'x'}, dimensions={0} | all-to-all | bytes 4194304 | tf_op jit(solution)/shard_map/w_in/all_to_all | solution.py:352
  68.4 2.1 %state.1 = (bf16[256,128]{1,0:T(8,128)(2,1)S(1)}, f32[256,256]{1,0:T(8,128)S(1)}, f32[256,128]{1,0:T(8,128)S(1)}, bf16[512,128]{1,0:T(8,128)(2,1)}, bf16[512,256]{1,0:T(8,128)(2,1)S(1)}) custom-call(bf16[256,2176]{1,0:T(8,128)(2,1)S(1)} %bitcast.24, bf16[4,512,512]{2,1,0:T(8,128)(2,1)S(1)} %all_to_all.42.w_ref, f32[256,128]{1,0:T(8,128)S(1)} %get-tuple-element.19.aux_ref, ...), custom_call_target="tpu_custom_call" | custom-call | tf_op jit(solution)/shard_map/state/pallas_call | solution.py:353
  70.6 8.5 %all-to-all-start.2 = ((bf16[64,8,128]{2,1,0:T(8,128)(2,1)}), bf16[64,8,128]{2,1,0:T(8,128)(2,1)S(1)}, u32[]{:S(2)}, u32[]{:S(2)}) async-start(bf16[64,8,128]{2,1,0:T(8,128)(2,1)} %bitcast.12), calls=%async_computation.2 | async-start | bytes 262144 | tf_op jit(solution)/shard_map/states_out/all_to_all | solution.py:369
  79.1 4.4 %collective-permute-start = (bf16[512,256]{1,0:T(8,128)(2,1)S(1)}, bf16[512,256]{1,0:T(8,128)(2,1)S(1)}, u32[]{:S(2)}, u32[]{:S(2)}) collective-permute-start(bf16[512,256]{1,0:T(8,128)(2,1)S(1)} %get-tuple-element.27.own_back_ref), channel_id=1, source_target_pairs={{0,16},{8,24},{16,0},{24,8},{1,17},{9,25},{17,1},{25,9},{2,18},{10... | collective-permute-start | bytes 786440 | tf_op jit(solution)/shard_map/over_two/ppermute | solution.py:375
  83.5 4.5 %collective-permute-done.over_two_ref = bf16[512,256]{1,0:T(8,128)(2,1)S(1)} collective-permute-done((bf16[512,256]{1,0:T(8,128)(2,1)S(1)}, bf16[512,256]{1,0:T(8,128)(2,1)S(1)}, u32[]{:S(2)}, u32[]{:S(2)}) %collective-permute-start) | collective-permute-done | bytes 262176 | tf_op jit(solution)/shard_map/over_two/ppermute | solution.py:375
  88.0 6.1 %all-to-all-done.2 = bf16[64,8,128]{2,1,0:T(8,128)(2,1)S(1)} async-done(((bf16[64,8,128]{2,1,0:T(8,128)(2,1)}), bf16[64,8,128]{2,1,0:T(8,128)(2,1)S(1)}, u32[]{:S(2)}, u32[]{:S(2)}) %all-to-all-start.2) | async-done | bytes 131104 | tf_op jit(solution)/shard_map/states_out/all_to_all | solution.py:369
  94.1 1.2 prefix.1
  95.3 2.2 %collective-permute-start.1 = (bf16[2,512,256]{2,1,0:T(8,128)(2,1)S(1)}, bf16[2,512,256]{2,1,0:T(8,128)(2,1)S(1)}, u32[]{:S(2)}, u32[]{:S(2)}) collective-permute-start(bf16[2,512,256]{2,1,0:T(8,128)(2,1)S(1)} %get-tuple-element.30.double_ref), channel_id=1, source_target_pairs={{0,8},{8,16},{16,24},{24,0},{1,9},{9,17},{17,25},{25,1},{2,10},{10... | collective-permute-start | bytes 1572872 | tf_op jit(solution)/shard_map/over_one/ppermute | solution.py:392
  97.5 9.1 %all-to-all-start.3 = ((f32[64,4,128]{2,1,0:T(4,128)}), f32[64,4,128]{2,1,0:T(4,128)S(1)}, u32[]{:S(2)}, u32[]{:S(2)}) async-start(f32[64,4,128]{2,1,0:T(4,128)} %bitcast.14), calls=%async_computation.3 | async-start | bytes 262144 | tf_op jit(solution)/shard_map/states_back/all_to_all | solution.py:390
  106.6 0.1 pad_add_fusion.head_ref
  106.6 14.9 %all-to-all-done.3 = f32[64,4,128]{2,1,0:T(4,128)S(1)} async-done(((f32[64,4,128]{2,1,0:T(4,128)}), f32[64,4,128]{2,1,0:T(4,128)S(1)}, u32[]{:S(2)}, u32[]{:S(2)}) %all-to-all-start.3) | async-done | bytes 131104 | tf_op jit(solution)/shard_map/states_back/all_to_all | solution.py:390
  121.5 0.0 collective-permute-done.1.next_ref
  121.6 0.0 copy-done
  121.6 1.8 %finish.1 = bf16[256,2048]{1,0:T(8,128)(2,1)S(1)} custom-call(s32[2]{0:T(128)S(1)} %pad_add_fusion.head_ref, bf16[256,128]{1,0:T(8,128)(2,1)S(1)} %get-tuple-element.23.query_ref, f32[256,256]{1,0:T(8,128)S(1)} %get-tuple-element.24.numer_ref, f32[256,128]{1,0:T(8,128)S(1)} %get-tuple-element.25.denom_ref, f32[256,128]{1,0:T(8,128)S(1)} %get-tuple-element.19.aux_ref, ...), custom_call_target="tpu_custom_call" | custom-call | tf_op jit(solution)/shard_map/finish/pallas_call | solution.py:394
  123.4 16.3 %all_to_all.43 = bf16[2,128,2048]{2,1,0:T(8,128)(2,1)S(1)} all-to-all(bf16[2,128,2048]{2,1,0:T(8,128)(2,1)S(1)} %bitcast.25), channel_id=1, replica_groups=mesh['z'=16,'x'=4,'c'=2,'y'=4] {'c'}, dimensions={0} | all-to-all | bytes 2097152 | tf_op jit(solution)/shard_map/heads/all_to_all | solution.py:415
  139.6 0.3 reduce_sum.24
  139.9 11.7 %all_to_all.44 = bf16[4,32,2048]{2,1,0:T(8,128)(2,1)S(1)} all-to-all(bf16[4,32,2048]{2,1,0:T(8,128)(2,1)S(1)} %bitcast.29), channel_id=1, replica_groups=mesh['z'=16,'x'=4,'c'=2,'y'=4] {'y'}, dimensions={0} | all-to-all | bytes 1048576 | tf_op jit(solution)/shard_map/owners/all_to_all | solution.py:420
  151.6 0.7 reduce_sum.25
  (8 shorter events, 0.0 us)
Async XLA Ops:
  0.0 13.0 %copy-start.3 = (bf16[16,256]{1,0:T(8,128)(2,1)S(1)}, bf16[16,256]{1,0:T(8,128)(2,1)}, u32[]{:S(2)}) copy-start(bf16[16,256]{1,0:T(8,128)(2,1)} %param.13) | copy-start | bytes 24580
  0.0 13.0 %copy-start.1 = (bf16[16,512]{1,0:T(8,128)(2,1)S(1)}, bf16[16,512]{1,0:T(8,128)(2,1)}, u32[]{:S(2)}) copy-start(bf16[16,512]{1,0:T(8,128)(2,1)} %param.15) | copy-start | bytes 49156
  0.0 13.0 %copy-start.4 = (bf16[16,256]{1,0:T(8,128)(2,1)S(1)}, bf16[16,256]{1,0:T(8,128)(2,1)}, u32[]{:S(2)}) copy-start(bf16[16,256]{1,0:T(8,128)(2,1)} %param.14) | copy-start | bytes 24580
  0.0 13.1 %copy-start.2 = (bf16[16,512]{1,0:T(8,128)(2,1)S(1)}, bf16[16,512]{1,0:T(8,128)(2,1)}, u32[]{:S(2)}) copy-start(bf16[16,512]{1,0:T(8,128)(2,1)} %param.21) | copy-start | bytes 49156
  2.7 41.6 %all-to-all-start = ((bf16[8,32,2176]{2,1,0:T(8,128)(2,1)}), bf16[8,32,2176]{2,1,0:T(8,128)(2,1)S(1)}, u32[]{:S(2)}, u32[]{:S(2)}) async-start(bf16[8,32,2176]{2,1,0:T(8,128)(2,1)} %prepare.1), calls=%async_computation | async-start | bytes 2228224 | tf_op jit(solution)/shard_map/rows/all_to_all | solution.py:311
  68.4 53.1 %copy-start = (bf16[2048]{0:T(1024)(128)(2,1)S(1)}, bf16[2048]{0:T(1024)(128)(2,1)}, u32[]{:S(2)}) copy-start(bf16[2048]{0:T(1024)(128)(2,1)} %param.20) | copy-start | bytes 12292
  70.6 23.5 %all-to-all-start.2 = ((bf16[64,8,128]{2,1,0:T(8,128)(2,1)}), bf16[64,8,128]{2,1,0:T(8,128)(2,1)S(1)}, u32[]{:S(2)}, u32[]{:S(2)}) async-start(bf16[64,8,128]{2,1,0:T(8,128)(2,1)} %bitcast.12), calls=%async_computation.2 | async-start | bytes 262144 | tf_op jit(solution)/shard_map/states_out/all_to_all | solution.py:369
  79.1 8.9 %collective-permute-start = (bf16[512,256]{1,0:T(8,128)(2,1)S(1)}, bf16[512,256]{1,0:T(8,128)(2,1)S(1)}, u32[]{:S(2)}, u32[]{:S(2)}) collective-permute-start(bf16[512,256]{1,0:T(8,128)(2,1)S(1)} %get-tuple-element.27.own_back_ref), channel_id=1, source_target_pairs={{0,16},{8,24},{16,0},{24,8},{1,17},{9,25},{17,1},{25,9},{2,18},{10... | collective-permute-start | bytes 786440 | tf_op jit(solution)/shard_map/over_two/ppermute | solution.py:375
  95.3 26.3 %collective-permute-start.1 = (bf16[2,512,256]{2,1,0:T(8,128)(2,1)S(1)}, bf16[2,512,256]{2,1,0:T(8,128)(2,1)S(1)}, u32[]{:S(2)}, u32[]{:S(2)}) collective-permute-start(bf16[2,512,256]{2,1,0:T(8,128)(2,1)S(1)} %get-tuple-element.30.double_ref), channel_id=1, source_target_pairs={{0,8},{8,16},{16,24},{24,0},{1,9},{9,17},{17,25},{25,1},{2,10},{10... | collective-permute-start | bytes 1572872 | tf_op jit(solution)/shard_map/over_one/ppermute | solution.py:392
  97.5 24.1 %all-to-all-start.3 = ((f32[64,4,128]{2,1,0:T(4,128)}), f32[64,4,128]{2,1,0:T(4,128)S(1)}, u32[]{:S(2)}, u32[]{:S(2)}) async-start(f32[64,4,128]{2,1,0:T(4,128)} %bitcast.14), calls=%async_computation.3 | async-start | bytes 262144 | tf_op jit(solution)/shard_map/states_back/all_to_all | solution.py:390

commit v4 on v3

--- a/solution.py
+++ b/solution.py
@@ -9,7 +9,6 @@
 SP = ("z", "x", "c")
 SP_TP = ("z", "x", "c", "y")
 ROWS = ("z", "x")
-HEADS = 8
 DK = 128
 DV = 256
 norm_floor = 0.1
@@ -77,12 +76,12 @@
 
 
 def gates_kernel(
-    head_ref, rows_ref, along_ref, pair_ref, aux_ref, facts_ref, copies_ref, own_back_ref
+    head_ref, rows_ref, along_ref, pair_ref, aux_ref, facts_ref, copies_ref, own_ref
 ):
     cut = copies_ref.shape[2]
     for k in range(copies_ref.shape[0]):
         copies_ref[k] = along_ref[:, :cut]
-    own_back_ref[...] = along_ref[:, cut:]
+    own_ref[...] = along_ref[:, cut:]
     head = head_ref[0]
     gates = rows_ref[:, -128:].astype(f32)
     length = gates.shape[0]
@@ -123,38 +122,43 @@
     return jnp.sum(jnp.where(lane_ids(aux.shape) == k, aux, 0.0), axis=1, keepdims=True)
 
 
-def state_kernel(
-    rows_ref,
-    w_ref,
-    aux_ref,
-    facts_ref,
-    pair_ref,
-    own_back_ref,
-    query_ref,
-    numer_ref,
-    denom_ref,
-    message_ref,
-    passed_ref,
-    buffer_ref,
-):
-    passed_ref[...] = own_back_ref[...]
-    length, width = rows_ref.shape[0], rows_ref.shape[1] - 128
+def projected(rows_ref, w_ref, start, stop, width):
     x_size = w_ref.shape[0]
     run = 32
-    total = jnp.zeros((length, w_ref.shape[2]), f32)
+    total = jnp.zeros((rows_ref.shape[0], stop - start), f32)
     for k in range(width // 256):
         parts = [
-            w_ref[x, z * run : (z + 1) * run, :] for z in (2 * k, 2 * k + 1) for x in range(x_size)
+            w_ref[x, z * run : (z + 1) * run, start:stop]
+            for z in (2 * k, 2 * k + 1)
+            for x in range(x_size)
         ]
         total = total + jnp.dot(
             rows_ref[:, k * 256 : (k + 1) * 256],
             jnp.concatenate(parts, axis=0),
             preferred_element_type=f32,
         )
-    query = total[:, :DK].astype(bf16)
-    query_ref[...] = query
-    key = (total[:, DK : 2 * DK] * (DK**-0.5)).astype(bf16)
-    value = total[:, 2 * DK :].astype(bf16)
+    return total
+
+
+def state_kernel(
+    rows_ref,
+    w_ref,
+    aux_ref,
+    facts_ref,
+    own_ref,
+    key_ref,
+    value_ref,
+    message_ref,
+    passed_ref,
+    buffer_ref,
+):
+    passed_ref[...] = own_ref[...]
+    width = rows_ref.shape[1] - 128
+    total = projected(rows_ref, w_ref, 0, DK + DV, width)
+    key = (total[:, :DK] * (DK**-0.5)).astype(bf16)
+    value = total[:, DK:].astype(bf16)
+    key_ref[...] = key
+    value_ref[...] = value
     scaled_key = key.astype(f32) * column_of(aux_ref[...], 3)
     state = jnp.dot(value.astype(f32).T, scaled_key, precision=highest, preferred_element_type=f32)
     vector = jnp.sum(scaled_key, axis=0, keepdims=True)
@@ -166,18 +170,22 @@
     for r in (6, 7):
         buffer_ref[pl.ds(r, peers, stride=8), :] = jnp.zeros((peers, DK), f32)
     message_ref[...] = buffer_ref[...].astype(bf16)
-    scores = lax.dot_general(query, key, (((1,), (1,)), ((), ())), preferred_element_type=f32)
-    weights = scores * pair_ref[...]
-    numer_ref[...] = jnp.dot(weights.astype(bf16), value, preferred_element_type=f32)
-    denom = jnp.sum(weights, axis=1, keepdims=True)
-    denom_ref[...] = jnp.broadcast_to(denom, denom_ref.shape)
 
 
 def prefix_kernel(
-    place_ref, arrived_ref, own_back_ref, over_two_ref, out_ref, entry_ref, double_ref, buffer_ref
+    place_ref,
+    arrived_ref,
+    before_ref,
+    behind_ref,
+    out_ref,
+    entry_ref,
+    upper_ref,
+    lower_ref,
+    buffer_ref,
 ):
-    double_ref[0] = own_back_ref[...]
-    double_ref[1] = over_two_ref[...]
+    half = upper_ref.shape[0]
+    upper_ref[...] = before_ref[:half, :]
+    lower_ref[...] = behind_ref[half:, :]
     place = place_ref[0]
     buffer_ref[...] = arrived_ref[...].astype(f32)
     peers = buffer_ref.shape[0] // 8
@@ -213,29 +221,44 @@
 
 def finish_kernel(
     head_ref,
-    query_ref,
-    numer_ref,
-    denom_ref,
+    rows_ref,
+    key_ref,
+    value_ref,
+    pair_ref,
     aux_ref,
     state_ref,
     entry_ref,
     gain_ref,
-    double_ref,
-    next_ref,
+    own_ref,
+    before_ref,
+    behind_ref,
+    upper_ref,
+    lower_ref,
     out_ref,
     w_ref,
 ):
     head = head_ref[0]
     my_x = head_ref[1]
-    for k in range(2):
-        w_ref[(my_x + 2 * k) % 4] = double_ref[k]
-        w_ref[(my_x + 3 + 2 * k) % 4] = next_ref[k]
+    half = upper_ref.shape[0]
+    w_ref[my_x] = own_ref[...]
+    w_ref[(my_x + 3) % 4] = before_ref[...]
+    w_ref[(my_x + 1) % 4] = behind_ref[...]
+    w_ref[(my_x + 2) % 4, :half, :] = upper_ref[...]
+    w_ref[(my_x + 2) % 4, half:, :] = lower_ref[...]
+    width = out_ref.shape[1]
+    query_low = projected(rows_ref, w_ref, 0, DK, width).astype(bf16)
+    scores = lax.dot_general(
+        query_low, key_ref[...], (((1,), (1,)), ((), ())), preferred_element_type=f32
+    )
+    weights = scores * pair_ref[...]
+    numer = jnp.dot(weights.astype(bf16), value_ref[...], preferred_element_type=f32)
+    denom = jnp.sum(weights, axis=1, keepdims=True)
     peers = 64
     count = state_ref.shape[0] // peers
     state = jnp.concatenate(
         [state_ref[pl.ds(r, peers, stride=count), :] for r in range(count)], axis=0
     )
-    query = query_ref[...].astype(f32)
+    query = query_low.astype(f32)
     left = lax.dot_general(
         query, state, (((1,), (1,)), ((), ())), precision=highest, preferred_element_type=f32
     )
@@ -243,13 +266,12 @@
     entry_top = entry_ref[1:2, 0:1]
     left_denom = jnp.sum(query * entry_vec, axis=1, keepdims=True)
     aux = aux_ref[...]
-    denom = denom_ref[:, 0:1]
     peak = column_of(aux, 1)
     carried = column_of(aux, 2) + entry_top
     top = jnp.maximum(peak, carried)
     own = jnp.exp(peak - top)
     old = jnp.exp(carried - top)
-    numer = own * numer_ref[...] + old * left
+    numer = own * numer + old * left
     denom = own * denom + old * left_denom
     hidden = numer / jnp.maximum(jnp.abs(denom), jnp.exp(-top))
     gains = gain_ref[...].astype(f32)
@@ -267,7 +289,9 @@
     run = 32
     for k in range(out_ref.shape[1] // 256):
         parts = [
-            w_ref[x, z * run : (z + 1) * run, :] for z in (2 * k, 2 * k + 1) for x in range(x_size)
+            w_ref[x, z * run : (z + 1) * run, DK:]
+            for z in (2 * k, 2 * k + 1)
+            for x in range(x_size)
         ]
         out_ref[:, k * 256 : (k + 1) * 256] = lax.dot_general(
             heads_out,
@@ -307,8 +331,7 @@
         out_specs=vmem,
         name="prepare",
     )(forget_bias, tokens, pre_gain.reshape(-1, 128), w_igate.T, w_fgate.T, gate_drift.T)
-    with jax.named_scope("rows"):
-        all_rows = lax.all_to_all(own_rows, ("c", "y"), split_axis=0, concat_axis=0, tiled=True)
+    all_rows = lax.all_to_all(own_rows, ("c", "y"), split_axis=0, concat_axis=0, tiled=True)
     all_rows = near(all_rows.reshape(-1, width + 128))
     length = all_rows.shape[0]
 
@@ -316,9 +339,9 @@
         [
             jnp.concatenate(
                 [
-                    w_query[:, c * DK : (c + 1) * DK],
                     w_key[:, c * DK : (c + 1) * DK],
                     w_value[:, c * DV : (c + 1) * DV],
+                    w_query[:, c * DK : (c + 1) * DK],
                     w_out[:, c * DV : (c + 1) * DV],
                 ],
                 axis=1,
@@ -326,100 +349,99 @@
             for c in range(2)
         ]
     )
-    with jax.named_scope("pair"):
-        both = lax.all_gather(pair, "c", axis=0, tiled=False)
+    both = lax.all_gather(pair, "c", axis=0, tiled=False)
     mine = lax.dynamic_index_in_dim(both, core, axis=1, keepdims=False)
     mine = mine.reshape(-1, mine.shape[2])
-    with jax.named_scope("along_z"):
-        along_z = lax.all_gather(mine, "z", axis=0, tiled=True)
-    cut = 2 * DK + DV
-
-    pair_decay, aux, facts, copies, own_back = pl.pallas_call(
+    along_z = lax.all_gather(mine, "z", axis=0, tiled=True)
+    cut = DK + DV
+
+    rest = (along_z.shape[0], along_z.shape[1] - cut)
+    pair_decay, aux, facts, copies, own_rest = pl.pallas_call(
         gates_kernel,
         out_shape=(
             pltpu.VMEM((length, length), f32),
             pltpu.VMEM((length, 128), f32),
             pltpu.VMEM((8, 128), f32),
             pltpu.VMEM((x_size, along_z.shape[0], cut), bf16),
-            pltpu.VMEM((along_z.shape[0], along_z.shape[1] - cut), bf16),
+            pltpu.VMEM(rest, bf16),
         ),
         in_specs=[smem, vmem, vmem],
         out_specs=(vmem,) * 5,
         compiler_params=limit,
         name="gates",
     )(head, all_rows, near(along_z))
-    with jax.named_scope("w_in"):
-        w_in = lax.all_to_all(copies, "x", split_axis=0, concat_axis=0, tiled=True)
-    query, numer, denom, message, own_back = pl.pallas_call(
+    w_in = lax.all_to_all(copies, "x", split_axis=0, concat_axis=0, tiled=True)
+    key, value, message, own_rest = pl.pallas_call(
         state_kernel,
         out_shape=(
             pltpu.VMEM((length, DK), bf16),
-            pltpu.VMEM((length, DV), f32),
-            pltpu.VMEM((length, 128), f32),
+            pltpu.VMEM((length, DV), bf16),
             pltpu.VMEM((peers * 8, DK), bf16),
-            pltpu.VMEM(own_back.shape, bf16),
+            pltpu.VMEM(rest, bf16),
         ),
-        in_specs=[vmem] * 6,
-        out_specs=(vmem,) * 5,
+        in_specs=[vmem] * 5,
+        out_specs=(vmem,) * 4,
         scratch_shapes=[pltpu.VMEM((peers * 8, DK), f32)],
         compiler_params=limit,
         name="state",
-    )(all_rows, near(w_in), aux, facts, pair_decay, own_back)
-    with jax.named_scope("states_out"):
-        arrived = lax.all_to_all(message, ROWS, split_axis=0, concat_axis=0, tiled=True)
+    )(all_rows, near(w_in), aux, facts, own_rest)
+    arrived = lax.all_to_all(message, ROWS, split_axis=0, concat_axis=0, tiled=True)
 
     def ring(d):
         return [(k, (k + d) % x_size) for k in range(x_size)]
 
-    with jax.named_scope("over_two"):
-        over_two = lax.ppermute(own_back, "x", ring(2))
-    slices, entry, double = pl.pallas_call(
+    before = near(lax.ppermute(own_rest, "x", ring(1)))
+    behind = near(lax.ppermute(own_rest, "x", ring(-1)))
+    half = (rest[0] // 2, rest[1])
+    slices, entry, upper, lower = pl.pallas_call(
         prefix_kernel,
         out_shape=(
             pltpu.VMEM((DV, DK), f32),
             pltpu.VMEM((8, 128), f32),
-            pltpu.VMEM((2,) + own_back.shape, bf16),
+            pltpu.VMEM(half, bf16),
+            pltpu.VMEM(half, bf16),
         ),
         in_specs=[smem, vmem, vmem, vmem],
-        out_specs=(vmem,) * 3,
+        out_specs=(vmem,) * 4,
         scratch_shapes=[pltpu.VMEM((peers * 8, DK), f32)],
         compiler_params=limit,
         name="prefix",
-    )(place, near(arrived), own_back, near(over_two))
-    with jax.named_scope("states_back"):
-        state = lax.all_to_all(slices, ROWS, split_axis=0, concat_axis=0, tiled=True)
-    with jax.named_scope("over_one"):
-        following = lax.ppermute(double, "x", ring(1))
+    )(place, near(arrived), before, behind)
+    state = lax.all_to_all(slices, ROWS, split_axis=0, concat_axis=0, tiled=True)
+    upper = near(lax.ppermute(upper, "x", ring(1)))
+    lower = near(lax.ppermute(lower, "x", ring(-1)))
     where = jnp.concatenate([head, lax.axis_index("x").astype(jnp.int32).reshape(1)])
     partial = pl.pallas_call(
         finish_kernel,
         out_shape=pltpu.VMEM((length, width), bf16),
-        in_specs=[smem] + [vmem] * 9,
+        in_specs=[smem] + [vmem] * 13,
         out_specs=vmem,
-        scratch_shapes=[pltpu.VMEM((x_size,) + own_back.shape, bf16)],
+        scratch_shapes=[pltpu.VMEM((x_size,) + rest, bf16)],
         compiler_params=limit,
         name="finish",
     )(
         where,
-        query,
-        numer,
-        denom,
+        all_rows,
+        key,
+        value,
+        pair_decay,
         aux,
         near(state),
         entry,
         head_gain.reshape(-1, 128),
-        double,
-        near(following),
-    )
-    with jax.named_scope("heads"):
-        halves = lax.all_to_all(
-            partial.reshape(2, -1, width), "c", split_axis=0, concat_axis=0, tiled=True
-        )
+        own_rest,
+        before,
+        behind,
+        upper,
+        lower,
+    )
+    halves = lax.all_to_all(
+        partial.reshape(2, -1, width), "c", split_axis=0, concat_axis=0, tiled=True
+    )
     joined = halves.astype(f32).sum(axis=0).astype(bf16)
-    with jax.named_scope("owners"):
-        pieces = lax.all_to_all(
-            joined.reshape(-1, rows, width), "y", split_axis=0, concat_axis=0, tiled=True
-        )
+    pieces = lax.all_to_all(
+        joined.reshape(-1, rows, width), "y", split_axis=0, concat_axis=0, tiled=True
+    )
     return pieces.astype(f32).sum(axis=0).astype(bf16)
 
 

time: 153 us -> 146 us (0.954)
  starting transfers between devices: 34.5 us -> 43.2 us
  waiting for transfers between devices: 25.5 us -> 17.3 us
  blocking collectives: 82.6 us -> 74.9 us
    all_to_all x1, waiting for transfers between devices: 14.9 us -> 5.28 us  [on_device(): lax.all_to_all(slices, ROWS, split_axis=0, concat_axis=0, tiled=True)]
    ppermute x2 -> x4, waiting for transfers between devices: 4.47 us -> 11.6 us  [the longest x1 5.43 us: on_device(): before = near(lax.ppermute(own_rest, 'x', ring(1)))]
    ppermute x2 -> x4, starting transfers between devices: 6.58 us -> 12.5 us  [the longest x1 4.13 us: on_device(): behind = near(lax.ppermute(own_rest, 'x', ring(-1)))]
    all_to_all x1, waiting for transfers between devices: 6.09 us -> 0.4 us  [on_device(): lax.all_to_all(message, ROWS, split_axis=0, concat_axis=0, tiled=True)]
    all_to_all x1, blocking collectives: 23.5 us -> 17.9 us  [on_device(): w_in = lax.all_to_all(copies, 'x', split_axis=0, concat_axis=0, tiled=True)]
    all_to_all x1, starting transfers between devices: 9.09 us -> 11.9 us  [on_device(): lax.all_to_all(slices, ROWS, split_axis=0, concat_axis=0, tiled=True)]
    all_to_all x1, blocking collectives: 16.3 us -> 14.4 us  [on_device(): lax.all_to_all(partial.reshape(2, -1, width), 'c', split_axis=0, concat_a...]
  transfers between devices with their start and end apart: 5 -> 7, of which waited for: 3 -> 6; matrix products, arithmetic and copies ran while one was open for 0% -> 0% of each run, Pallas kernels for 0% -> 0%
where the time goes in v4:
time: 146 us
  blocking collectives  74.9 us (51%)
  starting transfers between devices  43.2 us (30%)
  waiting for transfers between devices  17.3 us (12%)
  Pallas kernels  9.06 us (6%)
    all_gather x1, blocking collectives, on_device(): along_z = lax.all_gather(mine, 'z', axis=0, tiled=True)  29.3 us
    all_to_all x1, blocking collectives, on_device(): w_in = lax.all_to_all(copies, 'x', split_axis=0, concat_axis=0, tiled=True)  17.9 us
    all_to_all x1, blocking collectives, on_device(): lax.all_to_all(partial.reshape(2, -1, width), 'c', split_axis=0, concat_a...  14.4 us
    all_to_all x1, starting transfers between devices, on_device(): lax.all_to_all(slices, ROWS, split_axis=0, concat_axis=0, tiled=True)  11.9 us
    all_to_all x1, blocking collectives, on_device(): lax.all_to_all(joined.reshape(-1, rows, width), 'y', split_axis=0, concat...  11.5 us
    all_to_all x1, starting transfers between devices, on_device(): lax.all_to_all(own_rows, ('c', 'y'), split_axis=0, concat_axis=0, tiled=T...  10.3 us
    all_to_all x1, starting transfers between devices, on_device(): lax.all_to_all(message, ROWS, split_axis=0, concat_axis=0, tiled=True)  8.5 us
    ppermute x1, waiting for transfers between devices, on_device(): before = near(lax.ppermute(own_rest, 'x', ring(1)))  5.43 us
  transfers between devices with their start and end apart: 7, of which 6 were waited for; matrix products, arithmetic and copies ran while one was open for 0% of the time, Pallas kernels for 0%

profile of v4, /device:TPU:1, one launch (start us, length us, event | category | flops | bytes accessed | tf_op | source)
XLA Modules:
  0.0 145.9 jit_solution(137992701786110400)
XLA Ops:
  0.0 0.0 copy-start.3
  0.0 2.7 %prepare.1 = bf16[8,32,2176]{2,1,0:T(8,128)(2,1)} custom-call(f32[8]{0:T(128)} %bias_ref.1, bf16[32,2048]{1,0:T(8,128)(2,1)} %tokens_ref.1, bf16[16,128]{1,0:T(8,128)(2,1)} %bitcast.35, bf16[8,2048]{1,0:T(8,128)(2,1)} %bitcast.33, bf16[8,2048]{1,0:T(8,128)(2,1)} %bitcast.34, f32[8,128]{1,0:T(8,128)} %bitcast.36), custom_call_target="tpu_custom_call" | custom-call | tf_op jit(solution)/shard_map/prepare/pallas_call | solution.py:327
  2.7 10.3 %all-to-all-start = ((bf16[8,32,2176]{2,1,0:T(8,128)(2,1)}), bf16[8,32,2176]{2,1,0:T(8,128)(2,1)S(1)}, u32[]{:S(2)}, u32[]{:S(2)}) async-start(bf16[8,32,2176]{2,1,0:T(8,128)(2,1)} %prepare.1), calls=%async_computation | async-start | bytes 2228224 | tf_op jit(solution)/shard_map/all_to_all | solution.py:334
  13.0 0.0 copy-done.4
  13.0 0.0 copy-done.2
  13.1 0.0 copy-done.5
  13.1 0.0 copy-done.3
  13.1 1.9 %all-gather = bf16[4,16,768]{2,1,0:T(8,128)(2,1)S(1)} all-gather(bf16[2,16,768]{2,1,0:T(8,128)(2,1)S(1)} %pad_maximum_fusion), channel_id=2, replica_groups=mesh['z'=16,'x'=4,'c'=2,'y'=4] {'c'}, dimensions={0}, use_global_device_ids=true | all-gather | bytes 147456 | tf_op jit(solution)/shard_map/all_gather | solution.py:352
  15.0 29.3 %all_gather.11.along_ref = bf16[512,768]{1,0:T(8,128)(2,1)S(1)} all-gather(bf16[32,768]{1,0:T(8,128)(2,1)S(1)} %bitcast.32), channel_id=1, replica_groups=mesh['z'=16,'x'=4,'c'=2,'y'=4] {'z'}, dimensions={0}, use_global_device_ids=true | all-gather | bytes 835584 | tf_op jit(solution)/shard_map/all_gather | solution.py:355
  44.3 0.0 all-to-all-done
  44.3 0.6 gates.1
  44.9 17.9 %all_to_all.42.w_ref = bf16[4,512,384]{2,1,0:T(8,128)(2,1)S(1)} all-to-all(bf16[4,512,384]{2,1,0:T(8,128)(2,1)S(1)} %get-tuple-element.18), channel_id=1, replica_groups=mesh['z'=16,'x'=4,'c'=2,'y'=4] {'x'}, dimensions={0} | all-to-all | bytes 3145728 | tf_op jit(solution)/shard_map/all_to_all | solution.py:373
  62.8 2.1 %state.1 = (bf16[256,128]{1,0:T(8,128)(2,1)S(1)}, bf16[256,256]{1,0:T(8,128)(2,1)S(1)}, bf16[512,128]{1,0:T(8,128)(2,1)}, bf16[512,384]{1,0:T(8,128)(2,1)S(1)}) custom-call(bf16[256,2176]{1,0:T(8,128)(2,1)S(1)} %bitcast.24, bf16[4,512,384]{2,1,0:T(8,128)(2,1)S(1)} %all_to_all.42.w_ref, f32[256,128]{1,0:T(8,128)S(1)} %get-tuple-element.19.aux_ref, ...), custom_call_target="tpu_custom_call" | custom-call | tf_op jit(solution)/shard_map/state/pallas_call | solution.py:374
  64.9 8.5 %all-to-all-start.2 = ((bf16[64,8,128]{2,1,0:T(8,128)(2,1)}), bf16[64,8,128]{2,1,0:T(8,128)(2,1)S(1)}, u32[]{:S(2)}, u32[]{:S(2)}) async-start(bf16[64,8,128]{2,1,0:T(8,128)(2,1)} %bitcast.12), calls=%async_computation.2 | async-start | bytes 262144 | tf_op jit(solution)/shard_map/all_to_all | solution.py:388
  73.4 4.1 %collective-permute-start.1 = (bf16[512,384]{1,0:T(8,128)(2,1)S(1)}, bf16[512,384]{1,0:T(8,128)(2,1)S(1)}, u32[]{:S(2)}, u32[]{:S(2)}) collective-permute-start(bf16[512,384]{1,0:T(8,128)(2,1)S(1)} %get-tuple-element.26.own_ref), channel_id=1, source_target_pairs={{0,24},{8,0},{16,8},{24,16},{1,25},{9,1},{17,9},{25,17},{2,26},{10... | collective-permute-start | bytes 1179656 | tf_op jit(solution)/shard_map/ppermute | solution.py:394
  77.6 1.9 %collective-permute-start = (bf16[512,384]{1,0:T(8,128)(2,1)S(1)}, bf16[512,384]{1,0:T(8,128)(2,1)S(1)}, u32[]{:S(2)}, u32[]{:S(2)}) collective-permute-start(bf16[512,384]{1,0:T(8,128)(2,1)S(1)} %get-tuple-element.26.own_ref), channel_id=1, source_target_pairs={{0,8},{8,16},{16,24},{24,0},{1,9},{9,17},{17,25},{25,1},{2,10},{10... | collective-permute-start | bytes 1179656 | tf_op jit(solution)/shard_map/ppermute | solution.py:393
  79.5 3.1 %collective-permute-done.1.behind_ref = bf16[512,384]{1,0:T(8,128)(2,1)S(1)} collective-permute-done((bf16[512,384]{1,0:T(8,128)(2,1)S(1)}, bf16[512,384]{1,0:T(8,128)(2,1)S(1)}, u32[]{:S(2)}, u32[]{:S(2)}) %collective-permute-start.1) | collective-permute-done | bytes 393248 | tf_op jit(solution)/shard_map/ppermute | solution.py:394
  82.6 5.4 %collective-permute-done.before_ref = bf16[512,384]{1,0:T(8,128)(2,1)S(1)} collective-permute-done((bf16[512,384]{1,0:T(8,128)(2,1)S(1)}, bf16[512,384]{1,0:T(8,128)(2,1)S(1)}, u32[]{:S(2)}, u32[]{:S(2)}) %collective-permute-start) | collective-permute-done | bytes 393248 | tf_op jit(solution)/shard_map/ppermute | solution.py:393
  88.0 0.4 all-to-all-done.2
  88.4 1.3 prefix.1
  89.7 11.9 %all-to-all-start.3 = ((f32[64,4,128]{2,1,0:T(4,128)}), f32[64,4,128]{2,1,0:T(4,128)S(1)}, u32[]{:S(2)}, u32[]{:S(2)}) async-start(f32[64,4,128]{2,1,0:T(4,128)} %bitcast.14), calls=%async_computation.3 | async-start | bytes 262144 | tf_op jit(solution)/shard_map/all_to_all | solution.py:410
  101.6 2.9 %collective-permute-start.2 = (bf16[256,384]{1,0:T(8,128)(2,1)}, bf16[256,384]{1,0:T(8,128)(2,1)S(1)}, u32[]{:S(2)}, u32[]{:S(2)}) collective-permute-start(bf16[256,384]{1,0:T(8,128)(2,1)} %get-tuple-element.29), channel_id=1, source_target_pairs={{0,8},{8,16},{16,24},{24,0},{1,9},{9,17},{17,25},{25,1},{2,10},{10... | collective-permute-start | bytes 589832 | tf_op jit(solution)/shard_map/ppermute | solution.py:411
  104.6 3.6 %collective-permute-start.3 = (bf16[256,384]{1,0:T(8,128)(2,1)}, bf16[256,384]{1,0:T(8,128)(2,1)S(1)}, u32[]{:S(2)}, u32[]{:S(2)}) collective-permute-start(bf16[256,384]{1,0:T(8,128)(2,1)} %copy-done.1), channel_id=1, source_target_pairs={{0,24},{8,0},{16,8},{24,16},{1,25},{9,1},{17,9},{25,17},{2,26},{10... | collective-permute-start | bytes 589832 | tf_op jit(solution)/shard_map/ppermute | solution.py:412
  108.1 0.1 pad_add_fusion.head_ref
  108.2 1.4 collective-permute-done.2.upper_ref
  109.7 1.7 %collective-permute-done.3.lower_ref = bf16[256,384]{1,0:T(8,128)(2,1)S(1)} collective-permute-done((bf16[256,384]{1,0:T(8,128)(2,1)}, bf16[256,384]{1,0:T(8,128)(2,1)S(1)}, u32[]{:S(2)}, u32[]{:S(2)}) %collective-permute-start.3) | collective-permute-done | bytes 196640 | tf_op jit(solution)/shard_map/ppermute | solution.py:412
  111.3 5.3 %all-to-all-done.3 = f32[64,4,128]{2,1,0:T(4,128)S(1)} async-done(((f32[64,4,128]{2,1,0:T(4,128)}), f32[64,4,128]{2,1,0:T(4,128)S(1)}, u32[]{:S(2)}, u32[]{:S(2)}) %all-to-all-start.3) | async-done | bytes 131104 | tf_op jit(solution)/shard_map/all_to_all | solution.py:410
  116.6 2.3 %finish.1 = bf16[256,2048]{1,0:T(8,128)(2,1)S(1)} custom-call(s32[2]{0:T(128)S(1)} %pad_add_fusion.head_ref, bf16[256,2176]{1,0:T(8,128)(2,1)S(1)} %bitcast.25, bf16[256,128]{1,0:T(8,128)(2,1)S(1)} %get-tuple-element.22.key_ref, bf16[256,256]{1,0:T(8,128)(2,1)S(1)} %get-tuple-element.23.value_ref, f32[256,256]{1,0:T(8,128)S(1)} %get-tuple-element.24.pair_ref, ...), custom_call_target="tpu_custom_call" | custom-call | tf_op jit(solution)/shard_map/finish/pallas_call | solution.py:414
  119.0 14.4 %all_to_all.43 = bf16[2,128,2048]{2,1,0:T(8,128)(2,1)S(1)} all-to-all(bf16[2,128,2048]{2,1,0:T(8,128)(2,1)S(1)} %bitcast.26), channel_id=1, replica_groups=mesh['z'=16,'x'=4,'c'=2,'y'=4] {'c'}, dimensions={0} | all-to-all | bytes 2097152 | tf_op jit(solution)/shard_map/all_to_all | solution.py:438
  133.3 0.3 reduce_sum.24
  133.6 11.5 %all_to_all.44 = bf16[4,32,2048]{2,1,0:T(8,128)(2,1)S(1)} all-to-all(bf16[4,32,2048]{2,1,0:T(8,128)(2,1)S(1)} %bitcast.30), channel_id=1, replica_groups=mesh['z'=16,'x'=4,'c'=2,'y'=4] {'y'}, dimensions={0} | all-to-all | bytes 1048576 | tf_op jit(solution)/shard_map/all_to_all | solution.py:442
  145.2 0.7 reduce_sum.25
  (14 shorter events, 0.0 us)
Async XLA Ops:
  0.0 13.0 %copy-start.4 = (bf16[16,256]{1,0:T(8,128)(2,1)S(1)}, bf16[16,256]{1,0:T(8,128)(2,1)}, u32[]{:S(2)}) copy-start(bf16[16,256]{1,0:T(8,128)(2,1)} %param.13) | copy-start | bytes 24580
  0.0 13.0 %copy-start.2 = (bf16[16,512]{1,0:T(8,128)(2,1)S(1)}, bf16[16,512]{1,0:T(8,128)(2,1)}, u32[]{:S(2)}) copy-start(bf16[16,512]{1,0:T(8,128)(2,1)} %param.15) | copy-start | bytes 49156
  0.0 13.1 %copy-start.5 = (bf16[16,256]{1,0:T(8,128)(2,1)S(1)}, bf16[16,256]{1,0:T(8,128)(2,1)}, u32[]{:S(2)}) copy-start(bf16[16,256]{1,0:T(8,128)(2,1)} %param.14) | copy-start | bytes 24580
  0.0 13.1 %copy-start.3 = (bf16[16,512]{1,0:T(8,128)(2,1)S(1)}, bf16[16,512]{1,0:T(8,128)(2,1)}, u32[]{:S(2)}) copy-start(bf16[16,512]{1,0:T(8,128)(2,1)} %param.21) | copy-start | bytes 49156
  2.7 41.6 %all-to-all-start = ((bf16[8,32,2176]{2,1,0:T(8,128)(2,1)}), bf16[8,32,2176]{2,1,0:T(8,128)(2,1)S(1)}, u32[]{:S(2)}, u32[]{:S(2)}) async-start(bf16[8,32,2176]{2,1,0:T(8,128)(2,1)} %prepare.1), calls=%async_computation | async-start | bytes 2228224 | tf_op jit(solution)/shard_map/all_to_all | solution.py:334
  62.8 53.8 %copy-start = (bf16[2048]{0:T(1024)(128)(2,1)S(1)}, bf16[2048]{0:T(1024)(128)(2,1)}, u32[]{:S(2)}) copy-start(bf16[2048]{0:T(1024)(128)(2,1)} %param.20) | copy-start | bytes 12292
  64.9 23.5 %all-to-all-start.2 = ((bf16[64,8,128]{2,1,0:T(8,128)(2,1)}), bf16[64,8,128]{2,1,0:T(8,128)(2,1)S(1)}, u32[]{:S(2)}, u32[]{:S(2)}) async-start(bf16[64,8,128]{2,1,0:T(8,128)(2,1)} %bitcast.12), calls=%async_computation.2 | async-start | bytes 262144 | tf_op jit(solution)/shard_map/all_to_all | solution.py:388
  73.4 9.2 %collective-permute-start.1 = (bf16[512,384]{1,0:T(8,128)(2,1)S(1)}, bf16[512,384]{1,0:T(8,128)(2,1)S(1)}, u32[]{:S(2)}, u32[]{:S(2)}) collective-permute-start(bf16[512,384]{1,0:T(8,128)(2,1)S(1)} %get-tuple-element.26.own_ref), channel_id=1, source_target_pairs={{0,24},{8,0},{16,8},{24,16},{1,25},{9,1},{17,9},{25,17},{2,26},{10... | collective-permute-start | bytes 1179656 | tf_op jit(solution)/shard_map/ppermute | solution.py:394
  77.6 10.5 %collective-permute-start = (bf16[512,384]{1,0:T(8,128)(2,1)S(1)}, bf16[512,384]{1,0:T(8,128)(2,1)S(1)}, u32[]{:S(2)}, u32[]{:S(2)}) collective-permute-start(bf16[512,384]{1,0:T(8,128)(2,1)S(1)} %get-tuple-element.26.own_ref), channel_id=1, source_target_pairs={{0,8},{8,16},{16,24},{24,0},{1,9},{9,17},{17,25},{25,1},{2,10},{10... | collective-permute-start | bytes 1179656 | tf_op jit(solution)/shard_map/ppermute | solution.py:393
  89.7 11.9 %copy-start.1 = (bf16[256,384]{1,0:T(8,128)(2,1)}, bf16[256,384]{1,0:T(8,128)(2,1)S(1)}, u32[]{:S(2)}) copy-start(bf16[256,384]{1,0:T(8,128)(2,1)S(1)} %get-tuple-element.30) | copy-start | bytes 589828
  89.7 26.9 %all-to-all-start.3 = ((f32[64,4,128]{2,1,0:T(4,128)}), f32[64,4,128]{2,1,0:T(4,128)S(1)}, u32[]{:S(2)}, u32[]{:S(2)}) async-start(f32[64,4,128]{2,1,0:T(4,128)} %bitcast.14), calls=%async_computation.3 | async-start | bytes 262144 | tf_op jit(solution)/shard_map/all_to_all | solution.py:410
  101.6 8.0 %collective-permute-start.2 = (bf16[256,384]{1,0:T(8,128)(2,1)}, bf16[256,384]{1,0:T(8,128)(2,1)S(1)}, u32[]{:S(2)}, u32[]{:S(2)}) collective-permute-start(bf16[256,384]{1,0:T(8,128)(2,1)} %get-tuple-element.29), channel_id=1, source_target_pairs={{0,8},{8,16},{16,24},{24,0},{1,9},{9,17},{17,25},{25,1},{2,10},{10... | collective-permute-start | bytes 589832 | tf_op jit(solution)/shard_map/ppermute | solution.py:411
  104.6 6.8 %collective-permute-start.3 = (bf16[256,384]{1,0:T(8,128)(2,1)}, bf16[256,384]{1,0:T(8,128)(2,1)S(1)}, u32[]{:S(2)}, u32[]{:S(2)}) collective-permute-start(bf16[256,384]{1,0:T(8,128)(2,1)} %copy-done.1), channel_id=1, source_target_pairs={{0,24},{8,0},{16,8},{24,16},{1,25},{9,1},{17,9},{25,17},{2,26},{10... | collective-permute-start | bytes 589832 | tf_op jit(solution)/shard_map/ppermute | solution.py:412

commit v5 on v4

--- a/solution.py
+++ b/solution.py
@@ -11,6 +11,7 @@
 ROWS = ("z", "x")
 DK = 128
 DV = 256
+FIRST_ROWS = 320
 norm_floor = 0.1
 lowest_log = -1e30
 highest = lax.Precision.HIGHEST
@@ -76,12 +77,12 @@
 
 
 def gates_kernel(
-    head_ref, rows_ref, along_ref, pair_ref, aux_ref, facts_ref, copies_ref, own_ref
+    head_ref, rows_ref, along_ref, pair_ref, aux_ref, facts_ref, copies_ref, rest_ref
 ):
     cut = copies_ref.shape[2]
     for k in range(copies_ref.shape[0]):
         copies_ref[k] = along_ref[:, :cut]
-    own_ref[...] = along_ref[:, cut:]
+    rest_ref[...] = along_ref[:, cut:]
     head = head_ref[0]
     gates = rows_ref[:, -128:].astype(f32)
     length = gates.shape[0]
@@ -122,19 +123,23 @@
     return jnp.sum(jnp.where(lane_ids(aux.shape) == k, aux, 0.0), axis=1, keepdims=True)
 
 
-def projected(rows_ref, w_ref, start, stop, width):
-    x_size = w_ref.shape[0]
-    run = 32
+def weight_rows(pieces, k, start, stop):
+    parts = []
+    for z in (2 * k, 2 * k + 1):
+        at, piece = 32 * z, pieces[0]
+        if at >= piece.shape[1]:
+            at, piece = at - piece.shape[1], pieces[1]
+        for x in range(piece.shape[0]):
+            parts.append(piece[x, at : at + 32, start:stop])
+    return jnp.concatenate(parts, axis=0)
+
+
+def projected(rows_ref, pieces, start, stop, width):
     total = jnp.zeros((rows_ref.shape[0], stop - start), f32)
     for k in range(width // 256):
-        parts = [
-            w_ref[x, z * run : (z + 1) * run, start:stop]
-            for z in (2 * k, 2 * k + 1)
-            for x in range(x_size)
-        ]
         total = total + jnp.dot(
             rows_ref[:, k * 256 : (k + 1) * 256],
-            jnp.concatenate(parts, axis=0),
+            weight_rows(pieces, k, start, stop),
             preferred_element_type=f32,
         )
     return total
@@ -145,16 +150,19 @@
     w_ref,
     aux_ref,
     facts_ref,
-    own_ref,
+    rest_ref,
     key_ref,
     value_ref,
     message_ref,
-    passed_ref,
+    first_ref,
+    second_ref,
     buffer_ref,
 ):
-    passed_ref[...] = own_ref[...]
+    cut = first_ref.shape[0]
+    first_ref[...] = rest_ref[:cut, :]
+    second_ref[...] = rest_ref[cut:, :]
     width = rows_ref.shape[1] - 128
-    total = projected(rows_ref, w_ref, 0, DK + DV, width)
+    total = projected(rows_ref, (w_ref,), 0, DK + DV, width)
     key = (total[:, :DK] * (DK**-0.5)).astype(bf16)
     value = total[:, DK:].astype(bf16)
     key_ref[...] = key
@@ -175,17 +183,13 @@
 def prefix_kernel(
     place_ref,
     arrived_ref,
-    before_ref,
-    behind_ref,
+    second_ref,
     out_ref,
     entry_ref,
-    upper_ref,
-    lower_ref,
+    passed_ref,
     buffer_ref,
 ):
-    half = upper_ref.shape[0]
-    upper_ref[...] = before_ref[:half, :]
-    lower_ref[...] = behind_ref[half:, :]
+    passed_ref[...] = second_ref[...]
     place = place_ref[0]
     buffer_ref[...] = arrived_ref[...].astype(f32)
     peers = buffer_ref.shape[0] // 8
@@ -229,24 +233,13 @@
     state_ref,
     entry_ref,
     gain_ref,
-    own_ref,
-    before_ref,
-    behind_ref,
-    upper_ref,
-    lower_ref,
+    first_ref,
+    second_ref,
     out_ref,
-    w_ref,
 ):
     head = head_ref[0]
-    my_x = head_ref[1]
-    half = upper_ref.shape[0]
-    w_ref[my_x] = own_ref[...]
-    w_ref[(my_x + 3) % 4] = before_ref[...]
-    w_ref[(my_x + 1) % 4] = behind_ref[...]
-    w_ref[(my_x + 2) % 4, :half, :] = upper_ref[...]
-    w_ref[(my_x + 2) % 4, half:, :] = lower_ref[...]
     width = out_ref.shape[1]
-    query_low = projected(rows_ref, w_ref, 0, DK, width).astype(bf16)
+    query_low = projected(rows_ref, (first_ref, second_ref), 0, DK, width).astype(bf16)
     scores = lax.dot_general(
         query_low, key_ref[...], (((1,), (1,)), ((), ())), preferred_element_type=f32
     )
@@ -285,17 +278,10 @@
     )
     scale = lax.rsqrt(jnp.mean(hidden * hidden, axis=1, keepdims=True) + norm_floor)
     heads_out = (hidden * scale * gain).astype(bf16)
-    x_size = w_ref.shape[0]
-    run = 32
-    for k in range(out_ref.shape[1] // 256):
-        parts = [
-            w_ref[x, z * run : (z + 1) * run, DK:]
-            for z in (2 * k, 2 * k + 1)
-            for x in range(x_size)
-        ]
+    for k in range(width // 256):
         out_ref[:, k * 256 : (k + 1) * 256] = lax.dot_general(
             heads_out,
-            jnp.concatenate(parts, axis=0),
+            weight_rows((first_ref, second_ref), k, DK, DK + DV),
             (((1,), (1,)), ((), ())),
             preferred_element_type=f32,
         ).astype(bf16)
@@ -371,56 +357,48 @@
         name="gates",
     )(head, all_rows, near(along_z))
     w_in = lax.all_to_all(copies, "x", split_axis=0, concat_axis=0, tiled=True)
-    key, value, message, own_rest = pl.pallas_call(
+    first, second = ((n, rest[1]) for n in (FIRST_ROWS, rest[0] - FIRST_ROWS))
+    key, value, message, own_first, own_second = pl.pallas_call(
         state_kernel,
         out_shape=(
             pltpu.VMEM((length, DK), bf16),
             pltpu.VMEM((length, DV), bf16),
             pltpu.VMEM((peers * 8, DK), bf16),
-            pltpu.VMEM(rest, bf16),
+            pltpu.VMEM(first, bf16),
+            pltpu.VMEM(second, bf16),
         ),
         in_specs=[vmem] * 5,
-        out_specs=(vmem,) * 4,
+        out_specs=(vmem,) * 5,
         scratch_shapes=[pltpu.VMEM((peers * 8, DK), f32)],
         compiler_params=limit,
         name="state",
     )(all_rows, near(w_in), aux, facts, own_rest)
     arrived = lax.all_to_all(message, ROWS, split_axis=0, concat_axis=0, tiled=True)
-
-    def ring(d):
-        return [(k, (k + d) % x_size) for k in range(x_size)]
-
-    before = near(lax.ppermute(own_rest, "x", ring(1)))
-    behind = near(lax.ppermute(own_rest, "x", ring(-1)))
-    half = (rest[0] // 2, rest[1])
-    slices, entry, upper, lower = pl.pallas_call(
+    first_part = near(lax.all_gather(own_first, "x", axis=0, tiled=False))
+    slices, entry, own_second = pl.pallas_call(
         prefix_kernel,
         out_shape=(
             pltpu.VMEM((DV, DK), f32),
-            pltpu.VMEM((8, 128), f32),
-            pltpu.VMEM(half, bf16),
-            pltpu.VMEM(half, bf16),
+            jax.ShapeDtypeStruct((8, 128), f32),
+            pltpu.VMEM(second, bf16),
         ),
-        in_specs=[smem, vmem, vmem, vmem],
-        out_specs=(vmem,) * 4,
+        in_specs=[smem, vmem, vmem],
+        out_specs=(vmem,) * 3,
         scratch_shapes=[pltpu.VMEM((peers * 8, DK), f32)],
         compiler_params=limit,
         name="prefix",
-    )(place, near(arrived), before, behind)
+    )(place, near(arrived), own_second)
     state = lax.all_to_all(slices, ROWS, split_axis=0, concat_axis=0, tiled=True)
-    upper = near(lax.ppermute(upper, "x", ring(1)))
-    lower = near(lax.ppermute(lower, "x", ring(-1)))
-    where = jnp.concatenate([head, lax.axis_index("x").astype(jnp.int32).reshape(1)])
+    second_part = near(lax.all_gather(own_second, "x", axis=0, tiled=False))
     partial = pl.pallas_call(
         finish_kernel,
         out_shape=pltpu.VMEM((length, width), bf16),
-        in_specs=[smem] + [vmem] * 13,
+        in_specs=[smem] + [vmem] * 10,
         out_specs=vmem,
-        scratch_shapes=[pltpu.VMEM((x_size,) + rest, bf16)],
         compiler_params=limit,
         name="finish",
     )(
-        where,
+        head,
         all_rows,
         key,
         value,
@@ -428,12 +406,9 @@
         aux,
         near(state),
         entry,
-        head_gain.reshape(-1, 128),
-        own_rest,
-        before,
-        behind,
-        upper,
-        lower,
+        pltpu.with_memory_space_constraint(head_gain.reshape(-1, 128), pltpu.HBM),
+        first_part,
+        second_part,
     )
     halves = lax.all_to_all(
         partial.reshape(2, -1, width), "c", split_axis=0, concat_axis=0, tiled=True

time: 146 us -> 152 us (1.041)
  blocking collectives: 74.9 us -> 101 us
  starting transfers between devices: 43.2 us -> 23.4 us
  waiting for transfers between devices: 17.3 us -> 15 us
    all_gather x0 -> x2, blocking collectives: none -> 23 us  [the longest x1 12 us: on_device(): second_part = near(lax.all_gather(own_second, 'x', axis=0, tiled=False))]
    all_to_all x1, waiting for transfers between devices: 0.4 us -> 15 us  [on_device(): lax.all_to_all(message, ROWS, split_axis=0, concat_axis=0, tiled=True)]
    ppermute x4 -> x0, starting transfers between devices: 12.5 us -> none  [the longest x1 4.13 us: on_device(): behind = near(lax.ppermute(own_rest, 'x', ring(-1)))]
    ppermute x4 -> x0, waiting for transfers between devices: 11.6 us -> none  [the longest x1 5.43 us: on_device(): before = near(lax.ppermute(own_rest, 'x', ring(1)))]
    all_to_all x1, starting transfers between devices: 11.9 us -> 4.62 us  [on_device(): lax.all_to_all(slices, ROWS, split_axis=0, concat_axis=0, tiled=True)]
    all_to_all x1, waiting for transfers between devices: 5.28 us -> 0.01 us  [on_device(): lax.all_to_all(slices, ROWS, split_axis=0, concat_axis=0, tiled=True)]
    all_to_all x1, blocking collectives: 14.4 us -> 17.8 us  [on_device(): lax.all_to_all(partial.reshape(2, -1, width), 'c', split_axis=0, concat_a...]
  transfers between devices with their start and end apart: 7 -> 3, of which waited for: 6 -> 1; matrix products, arithmetic and copies ran while one was open for 0% -> 0% of each run, Pallas kernels for 0% -> 0%
where the time goes in v5:
time: 152 us; the launch traced here: 151 us
  blocking collectives  101 us (66%)
  starting transfers between devices  23.4 us (15%)
  waiting for transfers between devices  15 us (10%)
  Pallas kernels  8.98 us (6%)
    all_gather x1, blocking collectives, on_device(): along_z = lax.all_gather(mine, 'z', axis=0, tiled=True)  29.3 us
    all_to_all x1, blocking collectives, on_device(): w_in = lax.all_to_all(copies, 'x', split_axis=0, concat_axis=0, tiled=True)  17.9 us
    all_to_all x1, blocking collectives, on_device(): lax.all_to_all(partial.reshape(2, -1, width), 'c', split_axis=0, concat_a...  17.8 us
    all_to_all x1, waiting for transfers between devices, on_device(): lax.all_to_all(message, ROWS, split_axis=0, concat_axis=0, tiled=True)  15 us
    all_gather x1, blocking collectives, on_device(): second_part = near(lax.all_gather(own_second, 'x', axis=0, tiled=False))  12 us
    all_to_all x1, blocking collectives, on_device(): lax.all_to_all(joined.reshape(-1, rows, width), 'y', split_axis=0, concat...  11.6 us
    all_gather x1, blocking collectives, on_device(): first_part = near(lax.all_gather(own_first, 'x', axis=0, tiled=False))  11 us
    all_to_all x1, starting transfers between devices, on_device(): lax.all_to_all(own_rows, ('c', 'y'), split_axis=0, concat_axis=0, tiled=T...  10.3 us
  transfers between devices with their start and end apart: 3, of which 1 were waited for; matrix products, arithmetic and copies ran while one was open for 0% of the time, Pallas kernels for 0%

profile of v5, /device:TPU:1, one launch (start us, length us, event | category | flops | bytes accessed | tf_op | source)
XLA Modules:
  0.0 151.4 jit_solution(13979325493288431814)
XLA Ops:
  0.0 0.0 copy-start.4
  0.0 0.0 copy-start.2
  0.0 0.0 copy-start.5
  0.0 0.0 copy-start.3
  0.0 2.7 %prepare.1 = bf16[8,32,2176]{2,1,0:T(8,128)(2,1)} custom-call(f32[8]{0:T(128)} %bias_ref.1, bf16[32,2048]{1,0:T(8,128)(2,1)} %tokens_ref.1, bf16[16,128]{1,0:T(8,128)(2,1)} %bitcast.37, bf16[8,2048]{1,0:T(8,128)(2,1)} %bitcast.35, bf16[8,2048]{1,0:T(8,128)(2,1)} %bitcast.36, f32[8,128]{1,0:T(8,128)} %bitcast.38), custom_call_target="tpu_custom_call" | custom-call | tf_op jit(solution)/shard_map/prepare/pallas_call | solution.py:313
  2.7 10.3 %all-to-all-start = ((bf16[8,32,2176]{2,1,0:T(8,128)(2,1)}), bf16[8,32,2176]{2,1,0:T(8,128)(2,1)S(1)}, u32[]{:S(2)}, u32[]{:S(2)}) async-start(bf16[8,32,2176]{2,1,0:T(8,128)(2,1)} %prepare.1), calls=%async_computation | async-start | bytes 2228224 | tf_op jit(solution)/shard_map/all_to_all | solution.py:320
  13.0 0.0 copy-done.4
  13.0 0.0 copy-done.2
  13.0 0.0 copy-done.5
  13.1 0.0 copy-done.3
  13.1 1.9 %all-gather = bf16[4,16,768]{2,1,0:T(8,128)(2,1)S(1)} all-gather(bf16[2,16,768]{2,1,0:T(8,128)(2,1)S(1)} %pad_maximum_fusion), channel_id=2, replica_groups=mesh['z'=16,'x'=4,'c'=2,'y'=4] {'c'}, dimensions={0}, use_global_device_ids=true | all-gather | bytes 147456 | tf_op jit(solution)/shard_map/all_gather | solution.py:338
  15.0 29.3 %all_gather.23.along_ref = bf16[512,768]{1,0:T(8,128)(2,1)S(1)} all-gather(bf16[32,768]{1,0:T(8,128)(2,1)S(1)} %bitcast.34), channel_id=1, replica_groups=mesh['z'=16,'x'=4,'c'=2,'y'=4] {'z'}, dimensions={0}, use_global_device_ids=true | all-gather | bytes 835584 | tf_op jit(solution)/shard_map/all_gather | solution.py:341
  44.3 0.0 all-to-all-done
  44.3 0.6 gates.1
  44.9 17.9 %all_to_all.42.w_ref = bf16[4,512,384]{2,1,0:T(8,128)(2,1)S(1)} all-to-all(bf16[4,512,384]{2,1,0:T(8,128)(2,1)S(1)} %get-tuple-element.18), channel_id=1, replica_groups=mesh['z'=16,'x'=4,'c'=2,'y'=4] {'x'}, dimensions={0} | all-to-all | bytes 3145728 | tf_op jit(solution)/shard_map/all_to_all | solution.py:359
  62.8 2.1 %state.1 = (bf16[256,128]{1,0:T(8,128)(2,1)S(1)}, bf16[256,256]{1,0:T(8,128)(2,1)S(1)}, bf16[512,128]{1,0:T(8,128)(2,1)}, bf16[320,384]{1,0:T(8,128)(2,1)S(1)}, bf16[192,384]{1,0:T(8,128)(2,1)S(1)}) custom-call(bf16[256,2176]{1,0:T(8,128)(2,1)S(1)} %bitcast.25, bf16[4,512,384]{2,1,0:T(8,128)(2,1)S(1)} %all_to_all.42.w_ref, ...), custom_call_target="tpu_custom_call" | custom-call | tf_op jit(solution)/shard_map/state/pallas_call | solution.py:361
  64.9 8.5 %all-to-all-start.2 = ((bf16[64,8,128]{2,1,0:T(8,128)(2,1)}), bf16[64,8,128]{2,1,0:T(8,128)(2,1)S(1)}, u32[]{:S(2)}, u32[]{:S(2)}) async-start(bf16[64,8,128]{2,1,0:T(8,128)(2,1)} %bitcast.11), calls=%async_computation.2 | async-start | bytes 262144 | tf_op jit(solution)/shard_map/all_to_all | solution.py:376
  73.4 15.0 %all-to-all-done.2 = bf16[64,8,128]{2,1,0:T(8,128)(2,1)S(1)} async-done(((bf16[64,8,128]{2,1,0:T(8,128)(2,1)}), bf16[64,8,128]{2,1,0:T(8,128)(2,1)S(1)}, u32[]{:S(2)}, u32[]{:S(2)}) %all-to-all-start.2) | async-done | bytes 131104 | tf_op jit(solution)/shard_map/all_to_all | solution.py:376
  88.4 1.2 prefix.1
  89.6 0.0 copy-start
  89.7 0.6 copy-done
  90.2 4.6 %all-to-all-start.3 = ((f32[64,4,128]{2,1,0:T(4,128)}), f32[64,4,128]{2,1,0:T(4,128)S(1)}, u32[]{:S(2)}, u32[]{:S(2)}) async-start(f32[64,4,128]{2,1,0:T(4,128)} %bitcast.13), calls=%async_computation.3 | async-start | bytes 262144 | tf_op jit(solution)/shard_map/all_to_all | solution.py:391
  94.9 11.0 %all-gather.1 = bf16[1280,384]{1,0:T(8,128)(2,1)S(1)} all-gather(bf16[320,384]{1,0:T(8,128)(2,1)S(1)} %get-tuple-element.29), channel_id=3, replica_groups=mesh['z'=16,'x'=4,'c'=2,'y'=4] {'x'}, dimensions={0}, use_global_device_ids=true | all-gather | bytes 1228800 | tf_op jit(solution)/shard_map/all_gather | solution.py:377
  105.9 12.0 %all-gather.2 = bf16[768,384]{1,0:T(8,128)(2,1)S(1)} all-gather(bf16[192,384]{1,0:T(8,128)(2,1)S(1)} %get-tuple-element.30), channel_id=4, replica_groups=mesh['z'=16,'x'=4,'c'=2,'y'=4] {'x'}, dimensions={0}, use_global_device_ids=true | all-gather | bytes 737280 | tf_op jit(solution)/shard_map/all_gather | solution.py:392
  117.9 0.0 all-to-all-done.3
  117.9 0.0 copy-start.1
  117.9 0.7 copy-done.1
  118.5 2.3 %finish.1 = bf16[256,2048]{1,0:T(8,128)(2,1)S(1)} custom-call(s32[1]{0:T(128)} %bitcast.head_ref, bf16[256,2176]{1,0:T(8,128)(2,1)S(1)} %bitcast.26, bf16[256,128]{1,0:T(8,128)(2,1)S(1)} %get-tuple-element.22.key_ref, bf16[256,256]{1,0:T(8,128)(2,1)S(1)} %get-tuple-element.23.value_ref, f32[256,256]{1,0:T(8,128)S(1)} %get-tuple-element.24.pair_ref, ...), custom_call_target="tpu_custom_call" | custom-call | tf_op jit(solution)/shard_map/finish/pallas_call | solution.py:393
  120.9 17.8 %all_to_all.43 = bf16[2,128,2048]{2,1,0:T(8,128)(2,1)S(1)} all-to-all(bf16[2,128,2048]{2,1,0:T(8,128)(2,1)S(1)} %bitcast.27), channel_id=1, replica_groups=mesh['z'=16,'x'=4,'c'=2,'y'=4] {'c'}, dimensions={0} | all-to-all | bytes 2097152 | tf_op jit(solution)/shard_map/all_to_all | solution.py:413
  138.7 0.3 reduce_sum.24
  139.0 11.6 %all_to_all.44 = bf16[4,32,2048]{2,1,0:T(8,128)(2,1)S(1)} all-to-all(bf16[4,32,2048]{2,1,0:T(8,128)(2,1)S(1)} %bitcast.32), channel_id=1, replica_groups=mesh['z'=16,'x'=4,'c'=2,'y'=4] {'y'}, dimensions={0} | all-to-all | bytes 1048576 | tf_op jit(solution)/shard_map/all_to_all | solution.py:417
  150.7 0.7 reduce_sum.25
  (7 shorter events, 0.0 us)
Async XLA Ops:
  0.0 13.0 %copy-start.4 = (bf16[16,256]{1,0:T(8,128)(2,1)S(1)}, bf16[16,256]{1,0:T(8,128)(2,1)}, u32[]{:S(2)}) copy-start(bf16[16,256]{1,0:T(8,128)(2,1)} %param.13) | copy-start | bytes 24580
  0.0 13.0 %copy-start.2 = (bf16[16,512]{1,0:T(8,128)(2,1)S(1)}, bf16[16,512]{1,0:T(8,128)(2,1)}, u32[]{:S(2)}) copy-start(bf16[16,512]{1,0:T(8,128)(2,1)} %param.15) | copy-start | bytes 49156
  0.0 13.0 %copy-start.5 = (bf16[16,256]{1,0:T(8,128)(2,1)S(1)}, bf16[16,256]{1,0:T(8,128)(2,1)}, u32[]{:S(2)}) copy-start(bf16[16,256]{1,0:T(8,128)(2,1)} %param.14) | copy-start | bytes 24580
  0.0 13.1 %copy-start.3 = (bf16[16,512]{1,0:T(8,128)(2,1)S(1)}, bf16[16,512]{1,0:T(8,128)(2,1)}, u32[]{:S(2)}) copy-start(bf16[16,512]{1,0:T(8,128)(2,1)} %param.21) | copy-start | bytes 49156
  2.7 41.6 %all-to-all-start = ((bf16[8,32,2176]{2,1,0:T(8,128)(2,1)}), bf16[8,32,2176]{2,1,0:T(8,128)(2,1)S(1)}, u32[]{:S(2)}, u32[]{:S(2)}) async-start(bf16[8,32,2176]{2,1,0:T(8,128)(2,1)} %prepare.1), calls=%async_computation | async-start | bytes 2228224 | tf_op jit(solution)/shard_map/all_to_all | solution.py:320
  64.9 23.5 %all-to-all-start.2 = ((bf16[64,8,128]{2,1,0:T(8,128)(2,1)}), bf16[64,8,128]{2,1,0:T(8,128)(2,1)S(1)}, u32[]{:S(2)}, u32[]{:S(2)}) async-start(bf16[64,8,128]{2,1,0:T(8,128)(2,1)} %bitcast.11), calls=%async_computation.2 | async-start | bytes 262144 | tf_op jit(solution)/shard_map/all_to_all | solution.py:376
  89.6 0.6 copy-start
  90.2 27.6 %all-to-all-start.3 = ((f32[64,4,128]{2,1,0:T(4,128)}), f32[64,4,128]{2,1,0:T(4,128)S(1)}, u32[]{:S(2)}, u32[]{:S(2)}) async-start(f32[64,4,128]{2,1,0:T(4,128)} %bitcast.13), calls=%async_computation.3 | async-start | bytes 262144 | tf_op jit(solution)/shard_map/all_to_all | solution.py:391
  117.9 0.7 copy-start.1
